TPU v7x, 32 devices: a whole 2x2x4 slice. The times are simulated.
32 devices in a mesh: grp: 1, ep: 16 (over z, y, x), tp: 2 (over core).
Axes of the slice: x: 2, y: 2, z: 4, core: 2. Of those that a mesh axis runs over, the one named last changes fastest.
Arguments:
- layer_input: bfloat16 [512, 2048], P(('grp', 'ep')), may hold values from -6 to 6
- ssm_state: float32 [2, 512, 32, 64], P(None, ('grp', 'ep'), 'tp'), may hold values from -4 to 4
- w_input: bfloat16 [2048, 512], P(None, 'tp'), may hold values from -0.125 to 0.125
- decay_rate: float32 [32, 64], P('tp'), may hold values from 0.05 to 2
- frequency: float32 [32, 64], P('tp'), may hold values from 0 to 20
- step_log: float32 [32], P('tp'), may hold values from -2.3 to 0
- input_map: float32 [2, 32, 64, 16], P(None, 'tp'), may hold values from -1 to 1
- output_map: float32 [2, 32, 16, 64], P(None, 'tp'), may hold values from -0.75 to 0.75
- skip_gain: float32 [32, 16], P('tp'), may hold values from -3 to 3
- glu_weight: bfloat16 [512, 512], replicated, may hold values from -0.25 to 0.25
- mix_out: bfloat16 [512, 2048], replicated, may hold values from -0.75 to 0.75
- norm_gain: float32 [2048], replicated, may hold values from 0.1 to 6, as said below
- norm_shift: float32 [2048], replicated, may hold values from -2 to 2
- route_ids: int32 [512, 6], P(('grp', 'ep')), may hold values from 0 to 15, all different within a row; in each aligned block of 32 rows (0 to 31, 32 to 63, ...) at most 24 rows name the same one
- route_weights: float32 [512, 6], P(('grp', 'ep')), may hold values from 0.1 to 1
- gate_expert: bfloat16 [16, 2048, 512], P('ep', None, 'tp'), may hold values from -0.125 to 0.125
- up_expert: bfloat16 [16, 2048, 512], P('ep', None, 'tp'), may hold values from -0.125 to 0.125
- down_expert: bfloat16 [16, 512, 2048], P('ep', 'tp'), may hold values from -0.25 to 0.25
- gate_shared: bfloat16 [2048, 512], P(None, 'tp'), may hold values from -0.125 to 0.125
- up_shared: bfloat16 [2048, 512], P(None, 'tp'), may hold values from -0.125 to 0.125
- down_shared: bfloat16 [512, 2048], P('tp'), may hold values from -0.25 to 0.25
- dense_in: bfloat16 [1024, 2048], P('ep'), may hold values from -0.125 to 0.125
- dense_out: bfloat16 [1024, 2048], P('ep', 'tp'), may hold values from -0.1875 to 0.1875
- branch_gate: bfloat16 [2048], replicated, may hold values from -0.125 to 0.125
- final_gain: float32 [2048], P('tp'), may hold values from 0.1 to 1.9
- final_shift: float32 [2048], P('tp'), may hold values from -2 to 2
Outputs:
- layer_output: bfloat16 [512, 2048], P(('grp', 'ep'), 'tp')
- new_state: float32 [2, 512, 32, 64], P(None, ('grp', 'ep'), 'tp')
Inputs may be any that keep to these rules, and one draw needn't show every extreme that they name: `route_ids`: each row names 6 different experts; within each aligned block of 32 rows no expert is named more than 24 times, and in some block one expert is named exactly 24 times. `norm_gain`: positive gains.
All inputs are finite; a program needn't handle non-finite values.
Results may differ from a plain program's by a relative error of at most 0.015.
Values may be sent and summed in bfloat16 or wider, within the bound.
No kernel may reach another device: no remote copies, remote signals or barrier semaphores. Data moves between devices by JAX's collectives and lax.ppermute only.
A program may use at most 128 MiB of HBM per device.

v0:
```python
import jax
import jax.numpy as jnp
from jax import lax
from jax.sharding import PartitionSpec as P

residual_alpha = 1.681792830507429
route_scale = 2.5
norm_eps = 1e-05
highest = lax.Precision.HIGHEST


def state_update(
    inputs, ssm_state, decay_rate, frequency, step_log, input_map, output_map, skip_gain
):
    step_size = jnp.exp(step_log)[:, None]
    magnitude = jnp.exp(-decay_rate * step_size)
    rotation = frequency * step_size
    decay_re = magnitude * jnp.cos(rotation)
    decay_im = magnitude * jnp.sin(rotation)
    eigen_re = -decay_rate
    denominator = eigen_re * eigen_re + frequency * frequency
    factor_re = ((decay_re - 1.0) * eigen_re + decay_im * frequency) / denominator
    factor_im = (decay_im * eigen_re - (decay_re - 1.0) * frequency) / denominator
    drive_re = factor_re[..., None] * input_map[0] - factor_im[..., None] * input_map[1]
    drive_im = factor_re[..., None] * input_map[1] + factor_im[..., None] * input_map[0]
    pushed_re = jnp.einsum("gpm,tgm->tgp", drive_re, inputs, precision=highest)
    pushed_im = jnp.einsum("gpm,tgm->tgp", drive_im, inputs, precision=highest)
    new_re = decay_re * ssm_state[0] - decay_im * ssm_state[1] + pushed_re
    new_im = decay_re * ssm_state[1] + decay_im * ssm_state[0] + pushed_im
    response = (
        jnp.einsum("gmp,tgp->tgm", output_map[0], new_re, precision=highest)
        - jnp.einsum("gmp,tgp->tgm", output_map[1], new_im, precision=highest)
        + skip_gain * inputs
    )
    return (response, jnp.stack([new_re, new_im]))


def layer_norm_rows(values, gain, shift):
    mean = jnp.mean(values, axis=1, keepdims=True)
    variance = jnp.mean(jnp.square(values - mean), axis=1, keepdims=True)
    return (values - mean) * lax.rsqrt(variance + norm_eps) * gain + shift


def expert_terms(slot_rows, gate_weight, up_weight, down_weight):
    gate_part = jnp.einsum(
        "send,edf->senf", slot_rows, gate_weight, preferred_element_type=jnp.float32
    )
    up_part = jnp.einsum("send,edf->senf", slot_rows, up_weight, preferred_element_type=jnp.float32)
    hidden = (jax.nn.silu(gate_part) * up_part).astype(jnp.bfloat16)
    return jnp.einsum("senf,efd->send", hidden, down_weight, preferred_element_type=jnp.float32)


def finish_experts(partial_value):
    summed = lax.psum_scatter(
        partial_value.astype(jnp.bfloat16), "tp", scatter_dimension=3, tiled=True
    )
    return lax.all_to_all(summed, "ep", split_axis=0, concat_axis=0, tiled=True)


def dense_rows(rows, in_piece, out_piece):
    hidden = jax.nn.gelu(
        lax.dot_general(
            rows, in_piece, (((1,), (1,)), ((), ())), preferred_element_type=jnp.float32
        )
    ).astype(jnp.bfloat16)
    return jnp.dot(hidden, out_piece, preferred_element_type=jnp.float32)


def body(
    layer_input,
    ssm_state,
    w_input,
    decay_rate,
    frequency,
    step_log,
    input_map,
    output_map,
    skip_gain,
    glu_weight,
    mix_out,
    norm_gain,
    norm_shift,
    route_ids,
    route_weights,
    gate_expert,
    up_expert,
    down_expert,
    gate_shared,
    up_shared,
    down_shared,
    dense_in,
    dense_out,
    branch_gate,
    final_gain,
    final_shift,
):
    count_ep = lax.axis_size("ep")
    count_tp = lax.axis_size("tp")
    core = lax.axis_index("tp")
    seq_rows, width = layer_input.shape
    local_groups, channels = skip_gain.shape
    projected = jnp.dot(layer_input, w_input, preferred_element_type=jnp.float32).astype(
        jnp.bfloat16
    )
    inputs = projected.astype(jnp.float32).reshape(seq_rows, local_groups, channels)
    response, new_state = state_update(
        inputs, ssm_state, decay_rate, frequency, step_log, input_map, output_map, skip_gain
    )
    activated = jax.nn.gelu(response.reshape(seq_rows, local_groups * channels)).astype(
        jnp.bfloat16
    )
    every_channel = lax.all_gather(activated, "tp", axis=1, tiled=True)
    glu_out = (
        every_channel.astype(jnp.float32)
        * jax.nn.sigmoid(jnp.dot(every_channel, glu_weight, preferred_element_type=jnp.float32))
    ).astype(jnp.bfloat16)
    mixed = jnp.dot(glu_out, mix_out, preferred_element_type=jnp.float32).astype(jnp.bfloat16)
    normed = layer_norm_rows(
        residual_alpha * layer_input.astype(jnp.float32) + mixed.astype(jnp.float32),
        norm_gain,
        norm_shift,
    ).astype(jnp.bfloat16)
    top_k = route_ids.shape[1]
    local_experts = gate_expert.shape[0]
    experts = local_experts * count_ep
    capacity = count_tp * max(1, min(seq_rows // count_tp, seq_rows * top_k // experts))
    flat_ids = route_ids.reshape(-1)
    hits = (flat_ids[:, None] == jnp.arange(experts, dtype=jnp.int32)[None, :]).astype(jnp.int32)
    ranks = jnp.sum((jnp.cumsum(hits, axis=0) - hits) * hits, axis=1)
    target = flat_ids * capacity + ranks
    outgoing = (
        jnp.zeros((experts * capacity, width), jnp.bfloat16)
        .at[target]
        .set(jnp.repeat(normed, top_k, axis=0))
        .reshape(count_ep, local_experts, capacity, width)
    )
    returned = finish_experts(
        expert_terms(
            lax.all_to_all(outgoing, "ep", split_axis=0, concat_axis=0, tiled=True),
            gate_expert,
            up_expert,
            down_expert,
        )
    )
    half_width = returned.shape[3]
    picked = returned.reshape(experts * capacity, half_width)[target].astype(jnp.float32)
    weights = route_weights / jnp.sum(route_weights, axis=1, keepdims=True) * route_scale
    routed = jnp.sum(picked.reshape(seq_rows, top_k, half_width) * weights[:, :, None], axis=1)
    shared_gate = jnp.dot(normed, gate_shared, preferred_element_type=jnp.float32)
    shared_up = jnp.dot(normed, up_shared, preferred_element_type=jnp.float32)
    shared_hidden = (jax.nn.silu(shared_gate) * shared_up).astype(jnp.bfloat16)
    shared_part = jnp.dot(shared_hidden, down_shared, preferred_element_type=jnp.float32)
    shared = lax.psum_scatter(
        shared_part.astype(jnp.bfloat16), "tp", scatter_dimension=1, tiled=True
    )
    every_row = lax.all_gather(normed, "ep", axis=0, tiled=True)
    dense = lax.psum_scatter(
        dense_rows(every_row, dense_in, dense_out), "ep", scatter_dimension=0, tiled=True
    )
    own_normed = lax.dynamic_slice_in_dim(normed, core * half_width, half_width, 1).astype(
        jnp.float32
    )
    branch = jax.nn.sigmoid(jnp.dot(normed, branch_gate, preferred_element_type=jnp.float32))
    total = (
        residual_alpha * own_normed + routed + shared.astype(jnp.float32) + branch[:, None] * dense
    )
    row_sum, row_squares = lax.psum((jnp.sum(total, axis=1), jnp.sum(total * total, axis=1)), "tp")
    mean = row_sum / width
    variance = row_squares / width - mean * mean
    layer_output = (
        (total - mean[:, None]) * lax.rsqrt(variance[:, None] + norm_eps) * final_gain + final_shift
    ).astype(jnp.bfloat16)
    return (layer_output, new_state)


def solution(mesh):
    placed = (
        P(("grp", "ep"), None),
        P(None, ("grp", "ep"), "tp", None),
        P(None, "tp"),
        P("tp", None),
        P("tp", None),
        P("tp"),
        P(None, "tp", None, None),
        P(None, "tp", None, None),
        P("tp", None),
        P(),
        P(),
        P(),
        P(),
        P(("grp", "ep"), None),
        P(("grp", "ep"), None),
        P("ep", None, "tp"),
        P("ep", None, "tp"),
        P("ep", "tp", None),
        P(None, "tp"),
        P(None, "tp"),
        P("tp", None),
        P("ep", None),
        P("ep", "tp"),
        P(),
        P("tp"),
        P("tp"),
    )
    return jax.shard_map(
        body,
        mesh=mesh,
        in_specs=placed,
        out_specs=(P(("grp", "ep"), "tp"), P(None, ("grp", "ep"), "tp", None)),
        check_vma=False,
    )
```

profile of v0, /device:TPU:0, one launch (start us, length us, event | category | flops | bytes accessed | tf_op | source)
XLA Modules:
  0.0 209.7 jit_solution(1255208129824892549)
XLA Ops:
  8.1 1.7 convolution_convert_fusion.3
  11.8 0.5 fusion.25
  12.5 2.0 all_gather.6
  14.5 0.8 fusion.109
  15.5 0.8 add_convert_fusion
  16.5 0.6 reduce-window.6
  17.6 1.1 broadcast_in_dim.5
  18.7 1.1 reshape.143
  19.9 3.7 %scatter_custom_fusion = bf16[384,2048]{1,0:T(8,128)(2,1)} fusion(s32[192]{0:T(256)S(1)} %bitcast.168, bf16[192,2048]{1,0:T(8,128)(2,1)} %reshape.143, bf16[]{:T(256)} %constant.31.clone.1), kind=kCustom, calls=%fused_computation.42 | custom fusion | bytes 1573376 | tf_op jit(solution)/shard_map/scatter | solution.py:134
  23.6 58.4 %all_to_all.10 = bf16[16,1,24,2048]{3,2,1,0:T(8,128)(2,1)S(1)} all-to-all(bf16[16,1,24,2048]{3,2,1,0:T(8,128)(2,1)} %bitcast.160), channel_id=1, replica_groups=mesh['grp'=1,'ep'=16,'tp'=2] {'ep'}, dimensions={0} | all-to-all | bytes 3145728 | tf_op jit(solution)/shard_map/all_to_all | solution.py:139
  82.0 1.1 copy-done.1
  83.1 0.6 fusion.7
  83.7 5.1 %fusion = bf16[16,1,24,2048]{3,2,0,1:T(8,128)(2,1)} fusion(bf16[1,256,2048]{2,1,0:T(8,128)(2,1)} %param.43, bf16[16,1,24,2048]{3,2,1,0:T(8,128)(2,1)} %copy-done.1, bf16[1,2048,256]{2,1,0:T(8,128)(2,1)} %param.42, f32[16,1,24,256]{3,2,0,1:T(8,128)S(1)} %fusion.7), kind=kOutput, calls=%fused_computation.3 | convolution fusion | flops 806682624 | bytes 5636096 | tf_op jit(solution)/shard_map/senf,efd->send/dot_general | solution.py:50
  88.9 0.8 copy-done.2
  89.7 2.1 %fusion.112 = f32[32,256]{1,0:T(8,128)} fusion(bf16[32,2048]{1,0:T(8,128)(2,1)S(1)} %copy-done.2, bf16[2048,256]{1,0:T(8,128)(2,1)} %param.44), kind=kOutput, calls=%fused_computation.143 | convolution fusion | flops 33554432 | bytes 1212416 | tf_op jit(solution)/shard_map/dot_general | solution.py:149
  91.8 2.6 %convolution_convert_fusion.1 = bf16[32,2048]{1,0:T(8,128)(2,1)} fusion(bf16[256,2048]{1,0:T(8,128)(2,1)S(1)} %copy-done.6, bf16[32,2048]{1,0:T(8,128)(2,1)S(1)} %copy-done.2, bf16[2048,256]{1,0:T(8,128)(2,1)} %param.45, f32[32,256]{1,0:T(8,128)} %fusion.112), kind=kOutput, calls=%fused_computation.4 | convolution fusion | flops 67223552 | bytes 2392064 | tf_op jit(solution)/shard_map/dot_general | solution.py:152
  94.6 4.2 %fusion.72 = f32[512,1024]{1,0:T(8,128)} fusion(bf16[64,1024]{1,0:T(8,128)(2,1)} %param.48, bf16[512,2048]{1,0:T(8,128)(2,1)} %all-gather.2.cloned.1.call-done, bf16[64,2048]{1,0:T(8,128)(2,1)} %param.47), kind=kOutput, calls=%fused_computation.82 | convolution fusion | flops 201621504 | bytes 4587520 | tf_op jit(solution)/shard_map/dot_general | solution.py:66
  98.8 2.5 %reduce-scatter.4.cloned.1.call-done = bf16[16,1,24,1024]{3,2,0,1:T(8,128)(2,1)} async-done(((bf16[16,1,24,2048]{3,2,0,1:T(8,128)(2,1)}), bf16[16,1,24,1024]{3,2,0,1:T(8,128)(2,1)}) %reduce-scatter.4.cloned.1.call-update) | async-done | bytes 786448 | tf_op jit(solution)/shard_map/reduce_scatter | solution.py:54
  101.4 7.2 %all-to-all-start.1 = ((bf16[16,1,24,1024]{3,2,1,0:T(8,128)(2,1)}), bf16[16,1,24,1024]{3,2,1,0:T(8,128)(2,1)S(1)}, u32[]{:S(2)}, u32[]{:S(2)}) async-start(bf16[16,1,24,1024]{3,2,1,0:T(8,128)(2,1)} %bitcast.166), calls=%async_computation.2 | async-start | bytes 1572864 | tf_op jit(solution)/shard_map/all_to_all | solution.py:57
  108.6 0.6 reshape.150
  109.2 0.6 divide_multiply_fusion
  109.8 0.8 copy.67
  110.6 1.1 copy.68
  111.7 0.7 pad_clamp_fusion
  112.4 1.4 fusion.35
  113.8 16.0 %all-to-all-done.1 = bf16[16,1,24,1024]{3,2,1,0:T(8,128)(2,1)S(1)} async-done(((bf16[16,1,24,1024]{3,2,1,0:T(8,128)(2,1)}), bf16[16,1,24,1024]{3,2,1,0:T(8,128)(2,1)S(1)}, u32[]{:S(2)}, u32[]{:S(2)}) %all-to-all-start.1) | async-done | bytes 786464 | tf_op jit(solution)/shard_map/all_to_all | solution.py:57
  129.9 1.8 gather_fusion
  131.6 1.1 reshape.130
  133.2 63.9 %reduce-scatter.8.cloned.1.call-done = f32[32,1024]{1,0:T(8,128)} async-done(((f32[512,1024]{1,0:T(8,128)}), f32[32,1024]{1,0:T(8,128)}) %reduce-scatter.8.cloned.1.call-update) | async-done | bytes 131088 | tf_op jit(solution)/shard_map/reduce_scatter | solution.py:157
  197.1 1.1 fusion.107
  198.2 2.5 %all-reduce.1 = (f32[32]{0:T(128)S(1)}, f32[32]{0:T(128)S(1)}) all-reduce(f32[32]{0:T(128)S(1)} %get-tuple-element.9, f32[32]{0:T(128)S(1)} %get-tuple-element.8), channel_id=1, replica_groups=mesh['grp'=1,'ep'=16,'tp'=2] {'tp'}, use_global_device_ids=true, to_apply=%region_14.15 | all-reduce | flops 64 | bytes 512 | tf_op jit(solution)/shard_map/psum | solution.py:167
  200.7 1.4 add_convert_fusion.1
  (81 shorter events, 3.7 us)
Async XLA Ops:
  8.0 6.4 %copy-start = (bf16[512,2048]{1,0:T(8,128)(2,1)S(1)}, bf16[512,2048]{1,0:T(8,128)(2,1)}, u32[]{:S(2)}) copy-start(bf16[512,2048]{1,0:T(8,128)(2,1)} %param.36) | copy-start | bytes 6291460
  8.0 1.9 copy-start.9
  8.0 2.0 copy-start.21
  8.0 2.0 copy-start.15
  8.0 2.0 copy-start.16
  8.1 2.2 %copy-start.11 = (f32[2,16,64,16]{2,3,1,0:T(8,128)S(1)}, f32[2,16,64,16]{2,3,1,0:T(8,128)}, u32[]{:S(2)}) copy-start(f32[2,16,64,16]{2,3,1,0:T(8,128)} %param.32) | copy-start | bytes 393220
  8.1 86.5 %all-gather.2.cloned.1.call-start = ((), (), s32[]{:S(2)}) async-start(), calls=%async_computation.7 | async-start | bytes 2228224 | tf_op jit(solution)/shard_map/all_gather | solution.py:156
  10.0 1.1 copy-start.10
  10.0 1.8 copy-start.14
  10.2 4.2 %copy-start.7 = (bf16[512,512]{1,0:T(8,128)(2,1)S(1)}, bf16[512,512]{1,0:T(8,128)(2,1)}, u32[]{:S(2)}) copy-start(bf16[512,512]{1,0:T(8,128)(2,1)} %param.35) | copy-start | bytes 1572868
  10.2 4.2 %copy-start.8 = (bf16[32,2048]{1,0:T(8,128)(2,1)S(1)}, bf16[32,2048]{1,0:T(8,128)(2,1)}, u32[]{:S(2)}) copy-start(bf16[32,2048]{1,0:T(8,128)(2,1)} %param.26) | copy-start | bytes 393220
  11.1 0.7 copy-start.3
  14.4 1.0 copy-start.17
  14.5 1.0 copy-start.18
  14.5 1.9 copy-start.12
  16.3 85.1 %reduce-scatter.4.cloned.1.call-start = ((), (), s32[]{:S(2)}) async-start(), calls=%async_computation.5 | async-start | bytes 2359296 | tf_op jit(solution)/shard_map/reduce_scatter | solution.py:54
  19.9 3.7 %copy-start.20 = (s32[192,1]{0,1:T(1,128)}, s32[192,1]{0,1:T(1,128)S(1)}, u32[]{:S(2)}) copy-start(s32[192,1]{0,1:T(1,128)S(1)} %compare_select_fusion) | copy-start | bytes 2308
  23.6 59.6 %copy-start.5 = (bf16[1,2048,256]{2,1,0:T(8,128)(2,1)S(1)}, bf16[1,2048,256]{2,1,0:T(8,128)(2,1)}, u32[]{:S(2)}) copy-start(bf16[1,2048,256]{2,1,0:T(8,128)(2,1)} %param.41) | copy-start | bytes 3145732
  82.0 1.1 copy-start.1
  88.8 0.9 copy-start.2
  88.8 3.0 %copy-start.6 = (bf16[256,2048]{1,0:T(8,128)(2,1)S(1)}, bf16[256,2048]{1,0:T(8,128)(2,1)}, u32[]{:S(2)}) copy-start(bf16[256,2048]{1,0:T(8,128)(2,1)} %param.46) | copy-start | bytes 3145732
  88.8 44.3 %reduce-scatter.6.cloned.1.call-start = ((), (), s32[]{:S(2)}) async-start(), calls=%async_computation.6 | async-start | bytes 196608 | tf_op jit(solution)/shard_map/reduce_scatter | solution.py:153
  94.5 102.6 %reduce-scatter.8.cloned.1.call-start = ((), (), s32[]{:S(2)}) async-start(), calls=%async_computation.8 | async-start | bytes 2228224 | tf_op jit(solution)/shard_map/reduce_scatter | solution.py:157
  98.8 9.8 %copy-start.19 = (bf16[2048]{0:T(1024)(128)(2,1)S(1)}, bf16[2048]{0:T(1024)(128)(2,1)}, u32[]{:S(2)}) copy-start(bf16[2048]{0:T(1024)(128)(2,1)} %param.49) | copy-start | bytes 12292
  98.8 10.4 %copy-start.13 = (f32[32,6]{0,1:T(8,128)S(1)}, f32[32,6]{0,1:T(8,128)}, u32[]{:S(2)}) copy-start(f32[32,6]{0,1:T(8,128)} %param.40) | copy-start | bytes 2308
  98.8 11.8 %copy-start.4 = (f32[32,16,64]{2,0,1:T(8,128)S(1)}, f32[32,16,64]{2,0,1:T(8,128)}, u32[]{:S(2)}) copy-start(f32[32,16,64]{2,0,1:T(8,128)} %copy-done.3) | copy-start | bytes 393220
  101.4 28.5 %all-to-all-start.1 = ((bf16[16,1,24,1024]{3,2,1,0:T(8,128)(2,1)}), bf16[16,1,24,1024]{3,2,1,0:T(8,128)(2,1)S(1)}, u32[]{:S(2)}, u32[]{:S(2)}) async-start(bf16[16,1,24,1024]{3,2,1,0:T(8,128)(2,1)} %bitcast.166), calls=%async_computation.2 | async-start | bytes 1572864 | tf_op jit(solution)/shard_map/all_to_all | solution.py:57
Sparse Core Ops, SparseCore 0:
  16.4 71.7 all-gather.1
Sparse Core Ops, SparseCore 1:
  88.9 12.4 reduce-scatter.3
  103.4 8.8 reduce-scatter.5
  114.5 82.6 reduce-scatter.7
where the time goes:
time: 210 us
  waiting for transfers between devices  82.6 us (39%)
  blocking collectives  62.9 us (30%)
  matrix products  20.5 us (10%)
  between operations  16 us (8%)
  local copies, waits for them, and re-layouts  14.2 us (7%)
  starting transfers between devices  7.36 us (4%)
  other arithmetic  6.16 us (3%)
    reduce_scatter x1, waiting for transfers between devices, body(): lax.psum_scatter(dense_rows(every_row, dense_in, dense_out), 'ep', scatte...  63.9 us
    all_to_all x1, blocking collectives, body(): lax.all_to_all(outgoing, 'ep', split_axis=0, concat_axis=0, tiled=True)  58.4 us
    all_to_all x1, waiting for transfers between devices, finish_experts(): return lax.all_to_all(summed, 'ep', split_axis=0, concat_axis=0, tiled=True)  16 us
    all_to_all x1, starting transfers between devices, finish_experts(): return lax.all_to_all(summed, 'ep', split_axis=0, concat_axis=0, tiled=True)  7.19 us
    dot_general x1, matrix products, expert_terms(): jnp.einsum('senf,efd->send', hidden, down_weight, preferred_element_type=...  5.08 us
    dot_general x1, matrix products, dense_rows(): return jnp.dot(hidden, out_piece, preferred_element_type=jnp.float32)  4.24 us
  transfers between devices with their start and end apart: 5, of which 3 were waited for; matrix products, arithmetic and copies ran while one was open for 14% of the time, Pallas kernels for 0%

commit v1 on v0

v1 whole, which is shorter than its diff:
```python
import functools

import jax
import jax.numpy as jnp
from jax import lax
from jax.experimental import pallas as pl
from jax.experimental.pallas import tpu as pltpu
from jax.sharding import PartitionSpec as P


residual_alpha = 1.681792830507429
route_scale = 2.5
norm_eps = 1e-05
highest = lax.Precision.HIGHEST
both_axes = ("ep", "tp")


def state_update(
    inputs, ssm_state, decay_rate, frequency, step_log, input_map, output_map, skip_gain
):
    step_size = jnp.exp(step_log)[:, None]
    magnitude = jnp.exp(-decay_rate * step_size)
    rotation = frequency * step_size
    decay_re = magnitude * jnp.cos(rotation)
    decay_im = magnitude * jnp.sin(rotation)
    eigen_re = -decay_rate
    denominator = eigen_re * eigen_re + frequency * frequency
    factor_re = ((decay_re - 1.0) * eigen_re + decay_im * frequency) / denominator
    factor_im = (decay_im * eigen_re - (decay_re - 1.0) * frequency) / denominator
    drive_re = factor_re[..., None] * input_map[0] - factor_im[..., None] * input_map[1]
    drive_im = factor_re[..., None] * input_map[1] + factor_im[..., None] * input_map[0]
    pushed_re = jnp.einsum("gpm,tgm->tgp", drive_re, inputs, precision=highest)
    pushed_im = jnp.einsum("gpm,tgm->tgp", drive_im, inputs, precision=highest)
    new_re = decay_re * ssm_state[0] - decay_im * ssm_state[1] + pushed_re
    new_im = decay_re * ssm_state[1] + decay_im * ssm_state[0] + pushed_im
    response = (
        jnp.einsum("gmp,tgp->tgm", output_map[0], new_re, precision=highest)
        - jnp.einsum("gmp,tgp->tgm", output_map[1], new_im, precision=highest)
        + skip_gain * inputs
    )
    return (response, jnp.stack([new_re, new_im]))


def split_of(count_ep):
    inner = 1
    while inner < 4 and count_ep % (inner * 2) == 0:
        inner *= 2
    return (count_ep // inner, inner)


def outer_peer(place, step, outer):
    return place ^ step if outer & (outer - 1) == 0 else (place + step) % outer


def line_moves(step, count_ep, count_tp):
    outer, inner = split_of(count_ep)
    moves = []
    for rank in range(count_ep):
        peer = outer_peer(rank // inner, step, outer) * inner + rank % inner
        moves += [(rank * count_tp + t, peer * count_tp + t) for t in range(count_tp)]
    return moves


def plane_moves(step, count_ep, count_tp):
    moves = []
    for rank in range(count_ep):
        moves += [(rank * count_tp + t, (rank ^ step) * count_tp + t) for t in range(count_tp)]
    return moves


def backward(moves):
    return [(target, source) for source, target in moves]


vmem = pl.BlockSpec(memory_space=pltpu.VMEM)
smem = pl.BlockSpec(memory_space=pltpu.SMEM)
anywhere = pl.BlockSpec(memory_space=pl.ANY)


def product(left, right):
    return jnp.dot(left, right, preferred_element_type=jnp.float32)


def params(mebibytes):
    return pltpu.CompilerParams(vmem_limit_bytes=mebibytes << 20)


def cost(flops, moved):
    return pl.CostEstimate(flops=flops, bytes_accessed=moved, transcendentals=0)


def token_half(ref, flipped):
    half = ref.shape[0] // 2
    return jnp.where(flipped, ref[half:, :], ref[:half, :])


def mix_kernel(
    experts,
    core_ref,
    own_ref,
    far_ref,
    glu_ref,
    mix_ref,
    input_ref,
    gain_ref,
    shift_ref,
    ids_ref,
    scores_ref,
    packet_ref,
):
    width = input_ref.shape[1]
    flipped = core_ref[0] == 1
    own, far = token_half(own_ref, flipped), far_ref[...]
    every = jnp.concatenate([jnp.where(flipped, far, own), jnp.where(flipped, own, far)], axis=1)
    gated = (every.astype(jnp.float32) * jax.nn.sigmoid(product(every, glu_ref[...]))).astype(
        jnp.bfloat16
    )
    mixed = product(gated, mix_ref[...]).astype(jnp.bfloat16).astype(jnp.float32)
    values = residual_alpha * token_half(input_ref, flipped).astype(jnp.float32) + mixed
    mean = jnp.mean(values, axis=1, keepdims=True)
    centered = values - mean
    variance = jnp.mean(centered * centered, axis=1, keepdims=True)
    normed = centered * lax.rsqrt(variance + norm_eps) * gain_ref[...] + shift_ref[...]
    packet_ref[:, :width] = normed.astype(jnp.bfloat16)
    scores = token_half(scores_ref, flipped)
    ids = token_half(ids_ref, flipped)
    weights = scores / jnp.sum(scores, axis=1, keepdims=True) * route_scale
    rows, extra = packet_ref.shape[0], packet_ref.shape[1] - width
    lane = lax.broadcasted_iota(jnp.int32, (rows, extra), 1)
    expert = jnp.where(lane < experts, lane, lane - experts)
    spread = jnp.zeros((rows, extra), jnp.float32)
    for choice in range(scores.shape[1]):
        named = ids[:, choice : choice + 1] == expert
        spread = spread + jnp.where(named, weights[:, choice : choice + 1], 0.0)
    high = spread.astype(jnp.bfloat16).astype(jnp.float32)
    packet_ref[:, width:] = jnp.where(lane < experts, high, spread - high).astype(jnp.bfloat16)


def shared_kernel(own_ref, far_ref, gate_hbm, up_hbm, down_hbm, own_out, far_out, *scratch):
    gate_ref, up_ref, down_ref, sems = scratch
    copies = []
    for index, (source, target) in enumerate(zip((gate_hbm, up_hbm, down_hbm), scratch)):
        copies.append(pltpu.make_async_copy(source, target, sems.at[index]))
        copies[-1].start()
    width, half = own_out.shape[1], own_out.shape[0]
    normed = jnp.concatenate([own_ref[:, :width], far_ref[:, :width]], axis=0)
    copies[0].wait()
    gate_part = product(normed, gate_ref[...])
    copies[1].wait()
    hidden = (jax.nn.silu(gate_part) * product(normed, up_ref[...])).astype(jnp.bfloat16)
    copies[2].wait()
    result = product(hidden, down_ref[...]).astype(jnp.bfloat16)
    own_out[...] = result[:half]
    far_out[...] = result[half:]


def join_kernel(*refs):
    rows = refs[0].shape[0]
    for place, ref in enumerate(refs[:-1]):
        refs[-1][place * rows : (place + 1) * rows, :] = ref[...]


def sum_kernel(count, *refs):
    rows = refs[count].shape[0]
    for place, out_ref in enumerate(refs[count:]):
        total = refs[0][place * rows : (place + 1) * rows, :].astype(jnp.float32)
        for ref in refs[1:count]:
            total = total + ref[place * rows : (place + 1) * rows, :].astype(jnp.float32)
        out_ref[...] = total.astype(jnp.bfloat16)


def final_kernel(count, core_ref, packet_ref, own_norm_ref, far_norm_ref, *refs):
    own_ref, far_ref = refs[count:]
    half = own_ref.shape[1]
    flipped = core_ref[0] == 1
    total = residual_alpha * packet_ref[:, : 2 * half].astype(jnp.float32)
    for ref in refs[:count]:
        total = total + ref[...].astype(jnp.float32)
    mean = jnp.mean(total, axis=1, keepdims=True)
    variance = jnp.mean(total * total, axis=1, keepdims=True) - mean * mean
    scaled = (total - mean) * lax.rsqrt(variance + norm_eps)
    left, right = scaled[:, :half], scaled[:, half:]
    own = jnp.where(flipped, right, left)
    far = jnp.where(flipped, left, right)
    own_ref[...] = (own * own_norm_ref[:1] + own_norm_ref[1:]).astype(jnp.bfloat16)
    far_ref[...] = (far * far_norm_ref[:1] + far_norm_ref[1:]).astype(jnp.bfloat16)


def place_kernel(core_ref, own_ref, far_ref, out_ref):
    rows = own_ref.shape[0]
    flipped = core_ref[0] == 1
    own, far = own_ref[...], far_ref[...]
    out_ref[:rows, :] = jnp.where(flipped, far, own)
    out_ref[rows:, :] = jnp.where(flipped, own, far)


def routed_kernel(width, experts, local, place_ref, first_ref, second_ref, branch_ref, *refs):
    weights, outs = refs[:9], refs[9:11]
    held, sems = refs[11:20], refs[20]
    copies = [
        pltpu.make_async_copy(source, target, sems.at[index])
        for index, (source, target) in enumerate(zip(weights, held))
    ]
    for copy in copies:
        copy.start()
    own_expert, core = place_ref[0], place_ref[1]
    rows = jnp.concatenate([first_ref[...], second_ref[...]], axis=0)
    block = first_ref.shape[0]
    tokens = rows[:, :width]
    spread = rows[:, width:].astype(jnp.float32)
    lane = lax.broadcasted_iota(jnp.int32, spread.shape, 1)
    shares = []
    for index in range(local):
        chosen = (lane == own_expert + index) | (lane == own_expert + index + experts)
        shares.append(jnp.sum(jnp.where(chosen, spread, 0.0), axis=1, keepdims=True))
    logit = jnp.sum(
        tokens.astype(jnp.float32) * branch_ref[...].astype(jnp.float32), axis=1, keepdims=True
    )
    hidden = []
    for side in range(2):
        copies[2 * side].wait()
        copies[2 * side + 1].wait()
        for index in range(local):
            gate_part = product(tokens, held[2 * side][index])
            up_part = product(tokens, held[2 * side + 1][index])
            piece = jax.nn.silu(gate_part) * up_part * shares[index]
            hidden.append((piece.astype(jnp.bfloat16), held[4 + side], index))
    copies[6].wait()
    dense_part = lax.dot_general(
        tokens, held[6][...], (((1,), (1,)), ((), ())), preferred_element_type=jnp.float32
    )
    dense_hidden = (jax.nn.gelu(dense_part) * jax.nn.sigmoid(logit)).astype(jnp.bfloat16)
    for index in (4, 5, 7, 8):
        copies[index].wait()
    part = width // 2
    for side in range(2):
        own_side = core == side
        columns = jnp.where(own_side, held[7][...], held[8][...])
        for start in range(0, part, min(part, 512)):
            stop = min(start + 512, part)
            total = product(dense_hidden, columns[:, start:stop])
            low, high = side * part + start, side * part + stop
            for piece, down, index in hidden:
                total = total + product(piece, down[index, :, low:high])
            rounded = total.astype(jnp.bfloat16)
            outs[0][:, low:high] = rounded[:block]
            outs[1][:, low:high] = rounded[block:]


def routed_rows(width, place, first, second, branch_gate, experts, weights):
    rows = first.shape[0]
    return pl.pallas_call(
        functools.partial(routed_kernel, width, experts, weights[0].shape[0]),
        out_shape=[jax.ShapeDtypeStruct((rows, width), jnp.bfloat16)] * 2,
        in_specs=[smem, vmem, vmem, vmem] + [anywhere] * len(weights),
        out_specs=[vmem] * 2,
        scratch_shapes=[pltpu.VMEM(value.shape, value.dtype) for value in weights]
        + [pltpu.SemaphoreType.DMA((len(weights),))],
        compiler_params=params(28),
        cost_estimate=cost(24 * rows * weights[0].size, 8 << 20),
        name="routed_rows",
    )(place, first, second, branch_gate[None, :], *weights)


def body(
    layer_input,
    ssm_state,
    w_input,
    decay_rate,
    frequency,
    step_log,
    input_map,
    output_map,
    skip_gain,
    glu_weight,
    mix_out,
    norm_gain,
    norm_shift,
    route_ids,
    route_weights,
    gate_expert,
    up_expert,
    down_expert,
    gate_shared,
    up_shared,
    down_shared,
    dense_in,
    dense_out,
    branch_gate,
    final_gain,
    final_shift,
):
    count_ep = lax.axis_size("ep")
    count_tp = lax.axis_size("tp")
    core = lax.axis_index("tp")
    rank = lax.axis_index("ep")
    outer, inner = split_of(count_ep)
    seq_rows, width = layer_input.shape
    local_groups, channels = skip_gain.shape
    local_experts = gate_expert.shape[0]
    experts = local_experts * count_ep
    place = jnp.stack([rank * local_experts, core]).astype(jnp.int32)
    core_word = core.astype(jnp.int32)[None]

    def swapped(value):
        return lax.ppermute(value, "tp", [(t, 1 - t) for t in range(count_tp)])

    def moved(value, moves):
        return lax.ppermute(value, both_axes, moves)

    norm_own = jnp.stack([final_gain, final_shift])
    gate_far = swapped(gate_expert)
    up_far = swapped(up_expert)
    down_far = swapped(down_expert)
    dense_far = swapped(dense_out)
    norm_far = swapped(norm_own)
    projected = jnp.dot(layer_input, w_input, preferred_element_type=jnp.float32).astype(
        jnp.bfloat16
    )
    inputs = projected.astype(jnp.float32).reshape(seq_rows, local_groups, channels)
    response, new_state = state_update(
        inputs, ssm_state, decay_rate, frequency, step_log, input_map, output_map, skip_gain
    )
    activated = jax.nn.gelu(response.reshape(seq_rows, local_groups * channels)).astype(
        jnp.bfloat16
    )
    core_rows = seq_rows // count_tp
    far_tokens = lax.dynamic_slice_in_dim(activated, (1 - core) * core_rows, core_rows, 0)
    activated_far = swapped(far_tokens)
    packet_width = width + -(-2 * experts // 128) * 128
    packet_shape = jax.ShapeDtypeStruct((core_rows, packet_width), jnp.bfloat16)
    row_shape = jax.ShapeDtypeStruct((core_rows, width), jnp.bfloat16)
    packet = pl.pallas_call(
        functools.partial(mix_kernel, experts),
        out_shape=packet_shape,
        in_specs=[smem] + [vmem] * 9,
        out_specs=vmem,
        compiler_params=params(12),
        cost_estimate=cost(2 * seq_rows * (glu_weight.size + mix_out.size), 3 << 20),
        name="mix",
    )(
        core_word,
        activated,
        activated_far,
        glu_weight,
        mix_out,
        layer_input,
        norm_gain[None, :],
        norm_shift[None, :],
        route_ids,
        route_weights,
    )
    packet_far = swapped(packet)
    line = [packet]
    for step in range(1, outer):
        line.append(moved(packet, line_moves(step, count_ep, count_tp)))
    line = pl.pallas_call(
        join_kernel,
        out_shape=jax.ShapeDtypeStruct((outer * core_rows, packet_width), jnp.bfloat16),
        in_specs=[vmem] * outer,
        out_specs=vmem,
        compiler_params=params(12),
        cost_estimate=cost(outer * core_rows * packet_width, 1 << 20),
        name="join",
    )(*line)
    arrived = [line]
    for step in range(1, inner):
        arrived.append(moved(line, plane_moves(step, count_ep, count_tp)))
    held = (gate_shared, up_shared, down_shared)
    shared, shared_sent = pl.pallas_call(
        shared_kernel,
        out_shape=[row_shape] * 2,
        in_specs=[vmem] * 2 + [anywhere] * 3,
        out_specs=[vmem] * 2,
        scratch_shapes=[pltpu.VMEM(value.shape, value.dtype) for value in held]
        + [pltpu.SemaphoreType.DMA((3,))],
        compiler_params=params(12),
        cost_estimate=cost(6 * seq_rows * gate_shared.size, 3 << 20),
        name="shared_mlp",
    )(packet, packet_far, *held)
    shared_far = swapped(shared_sent)
    weights = [gate_expert, up_expert, gate_far, up_far, down_expert, down_far]
    weights += [dense_in, dense_out, dense_far]
    results = []
    for slot in range(inner // 2):
        first, second = arrived[slot * 2 : slot * 2 + 2]
        results += routed_rows(width, place, first, second, branch_gate, experts, weights)
    parts = [results[0]]
    for step in range(1, inner):
        moves = backward(plane_moves(step, count_ep, count_tp))
        parts.append(moved(results[step], moves))
    blocks = pl.pallas_call(
        functools.partial(sum_kernel, inner),
        out_shape=[row_shape] * outer,
        in_specs=[vmem] * inner,
        out_specs=[vmem] * outer,
        compiler_params=params(12),
        cost_estimate=cost(inner * outer * core_rows * width, 3 << 20),
        name="total",
    )(*parts)
    terms = [blocks[0]]
    for step in range(1, outer):
        moves = backward(line_moves(step, count_ep, count_tp))
        terms.append(moved(blocks[step], moves))
    half_shape = jax.ShapeDtypeStruct((core_rows, width // count_tp), jnp.bfloat16)
    terms += [shared, shared_far]
    own_half, far_half = pl.pallas_call(
        functools.partial(final_kernel, len(terms)),
        out_shape=[half_shape] * 2,
        in_specs=[smem] + [vmem] * (3 + len(terms)),
        out_specs=[vmem] * 2,
        compiler_params=params(12),
        cost_estimate=cost(10 * core_rows * width, 1 << 20),
        name="final",
    )(core_word, packet, norm_own, norm_far, *terms)
    handed = swapped(far_half)
    layer_output = pl.pallas_call(
        place_kernel,
        out_shape=jax.ShapeDtypeStruct((seq_rows, width // count_tp), jnp.bfloat16),
        in_specs=[smem, vmem, vmem],
        out_specs=vmem,
        compiler_params=params(12),
        cost_estimate=cost(seq_rows * width, 1 << 18),
        name="place",
    )(core_word, own_half, handed)
    return (layer_output, new_state)


def solution(mesh):
    placed = (
        P(("grp", "ep"), None),
        P(None, ("grp", "ep"), "tp", None),
        P(None, "tp"),
        P("tp", None),
        P("tp", None),
        P("tp"),
        P(None, "tp", None, None),
        P(None, "tp", None, None),
        P("tp", None),
        P(),
        P(),
        P(),
        P(),
        P(("grp", "ep"), None),
        P(("grp", "ep"), None),
        P("ep", None, "tp"),
        P("ep", None, "tp"),
        P("ep", "tp", None),
        P(None, "tp"),
        P(None, "tp"),
        P("tp", None),
        P("ep", None),
        P("ep", "tp"),
        P(),
        P("tp"),
        P("tp"),
    )
    return jax.shard_map(
        body,
        mesh=mesh,
        in_specs=placed,
        out_specs=(P(("grp", "ep"), "tp"), P(None, ("grp", "ep"), "tp", None)),
        check_vma=False,
    )
```

time: 210 us -> 78.6 us (0.37)
  blocking collectives: 62.9 us -> 0 us
  waiting for transfers between devices: 82.6 us -> 21.9 us
  starting transfers between devices: 7.36 us -> 24.3 us
  matrix products: 20.5 us -> 4.8 us
  between operations: 16 us -> 1.06 us
  Pallas kernels: 0 us -> 11.9 us
  other arithmetic: 6.16 us -> 0.29 us
    reduce_scatter x3 -> x0, waiting for transfers between devices: 66.5 us -> none  [the longest x1 63.9 us: body(): lax.psum_scatter(dense_rows(every_row, dense_in, dense_out), 'ep', scatte...]
    all_to_all x1 -> x0, blocking collectives: 58.4 us -> none  [body(): lax.all_to_all(outgoing, 'ep', split_axis=0, concat_axis=0, tiled=True)]
    ppermute x0 -> x21, starting transfers between devices: none -> 24.3 us  [the longest x12 22.7 us: moved(): return lax.ppermute(value, both_axes, moves)]
    ppermute x0 -> x21, waiting for transfers between devices: none -> 21.9 us  [the longest x12 17 us: moved(): return lax.ppermute(value, both_axes, moves)]
    dot_general x7 -> x0, matrix products: 16.8 us -> none  [the longest x1 5.08 us: expert_terms(): jnp.einsum('senf,efd->send', hidden, down_weight, preferred_element_type=...]
    all_to_all x1 -> x0, waiting for transfers between devices: 16 us -> none  [finish_experts(): return lax.all_to_all(summed, 'ep', split_axis=0, concat_axis=0, tiled=True)]
    pallas_call x0 -> x8, Pallas kernels: none -> 11.9 us  [the longest x2 8.86 us: routed_rows(): pl.pallas_call(functools.partial(routed_kernel, width, experts, weights[0...]
    all_to_all x1 -> x0, starting transfers between devices: 7.19 us -> none  [finish_experts(): return lax.all_to_all(summed, 'ep', split_axis=0, concat_axis=0, tiled=True)]
  transfers between devices with their start and end apart: 5 -> 21, of which waited for: 3 -> 12; matrix products, arithmetic and copies ran while one was open for 14% -> 12% of each run, Pallas kernels for 0% -> 14%
where the time goes in v1:
time: 78.6 us; the launch traced here: 78.1 us
  starting transfers between devices  24.3 us (31%)
  waiting for transfers between devices  21.9 us (28%)
  local copies, waits for them, and re-layouts  13.9 us (18%)
  Pallas kernels  11.9 us (15%)
  matrix products  4.8 us (6%)
  between operations  1.06 us (1%)
    ppermute x12, starting transfers between devices, moved(): return lax.ppermute(value, both_axes, moves)  22.7 us
    ppermute x12, waiting for transfers between devices, moved(): return lax.ppermute(value, both_axes, moves)  17 us
    unnamed x75, local copies, waits for them, and re-layouts  11 us
    pallas_call x2, Pallas kernels, routed_rows(): pl.pallas_call(functools.partial(routed_kernel, width, experts, weights[0...  8.86 us
    ppermute x9, waiting for transfers between devices, swapped(): return lax.ppermute(value, 'tp', [(t, 1 - t) for t in range(count_tp)])  4.92 us
    dot_general x1, matrix products, state_update(): jnp.einsum('gmp,tgp->tgm', output_map[1], new_im, precision=highest)  2.24 us
    ppermute x9, starting transfers between devices, swapped(): return lax.ppermute(value, 'tp', [(t, 1 - t) for t in range(count_tp)])  1.58 us
  transfers between devices with their start and end apart: 21, of which 12 were waited for; matrix products, arithmetic and copies ran while one was open for 12% of the time, Pallas kernels for 14%

profile of v1, /device:TPU:0, one launch (start us, length us, event | category | flops | bytes accessed | tf_op | source)
XLA Modules:
  0.0 78.1 jit_solution(4853703722945229638)
XLA Ops:
  2.4 1.1 %fusion.29 = (f32[1,32,16,64]{3,2,1,0:T(8,128)S(1)}, f32[1,32,16,64]{3,2,1,0:T(8,128)S(1)}) fusion(f32[2,32,16,64]{3,2,1,0:T(8,128)} %param.27), kind=kLoop, calls=%fused_computation.48 | loop fusion | bytes 524288 | tf_op jit(solution)/shard_map/slice | solution.py:34
  3.5 1.2 %convolution_convert_fusion = bf16[32,256]{1,0:T(8,128)(2,1)S(1)} fusion(bf16[32,2048]{1,0:T(8,128)(2,1)} %input_ref.1, bf16[2048,256]{1,0:T(8,128)(2,1)S(1)} %copy-done), kind=kOutput, calls=%fused_computation.7 | convolution fusion | flops 33562624 | bytes 1196032 | tf_op jit(solution)/shard_map/dot_general | solution.py:317
  7.2 2.2 %fusion.3 = f32[32,16,16]{0,2,1:T(8,128)} fusion(f32[16,32,16]{1,2,0:T(8,128)S(1)} %fusion.5, f32[32,16,64]{2,0,1:T(8,128)S(1)} %fusion, bf16[32,16,16]{0,2,1:T(8,128)(2,1)S(1)} %bitcast.70, f32[2,16,16,64]{3,2,1,0:T(8,128)} %param.33, f32[16,16]{1,0:T(8,128)S(1)} %copy-done.28), kind=kOutput, calls=%fused_computation.6 | convolution fusion | flops 6324224 | bytes 345088 | tf_op jit(solution)/shard_map/gmp,tgp->tgm/dot_general | solution.py:38
  9.5 1.0 %copy.44 = f32[32,256]{1,0:T(8,128)S(1)} copy(f32[32,256]{0,1:T(8,128)} %bitcast.71) | data formatting | bytes 65536 | tf_op jit(solution)/shard_map/reshape | solution.py:324
  11.7 1.6 %copy-done.5 = bf16[512,2048]{1,0:T(8,128)(2,1)S(1)} copy-done((bf16[512,2048]{1,0:T(8,128)(2,1)S(1)}, bf16[512,2048]{1,0:T(8,128)(2,1)}, u32[]{:S(2)}) %copy-start.5) | copy-done | bytes 2097176
  13.3 1.0 %copy-done.16 = bf16[512,512]{1,0:T(8,128)(2,1)S(1)} copy-done((bf16[512,512]{1,0:T(8,128)(2,1)S(1)}, bf16[512,512]{1,0:T(8,128)(2,1)}, u32[]{:S(2)}) %copy-start.16) | copy-done | bytes 524312
  15.1 2.8 %collective-permute-start.2 = (bf16[16,2176]{1,0:T(8,128)(2,1)S(1)}, bf16[16,2176]{1,0:T(8,128)(2,1)S(1)}, u32[]{:S(2)}, u32[]{:S(2)}) collective-permute-start(bf16[16,2176]{1,0:T(8,128)(2,1)S(1)} %mix.1.refs_0_.own_ref.packet_ref), channel_id=1, source_target_pairs={{0,8},{1,9},{2,10},{3,11},{4,12},{5,13},{6,14},{7,15},{8,0},{9,1},... | collective-permute-start | bytes 208904 | tf_op jit(solution)/shard_map/ppermute | solution.py:309
  17.9 2.6 %collective-permute-start.3 = (bf16[16,2176]{1,0:T(8,128)(2,1)S(1)}, bf16[16,2176]{1,0:T(8,128)(2,1)S(1)}, u32[]{:S(2)}, u32[]{:S(2)}) collective-permute-start(bf16[16,2176]{1,0:T(8,128)(2,1)S(1)} %mix.1.refs_0_.own_ref.packet_ref), channel_id=1, source_target_pairs={{0,16},{1,17},{2,18},{3,19},{4,20},{5,21},{6,22},{7,23},{8,24},{9,... | collective-permute-start | bytes 208904 | tf_op jit(solution)/shard_map/ppermute | solution.py:309
  20.6 4.7 %collective-permute-start.4 = (bf16[16,2176]{1,0:T(8,128)(2,1)S(1)}, bf16[16,2176]{1,0:T(8,128)(2,1)S(1)}, u32[]{:S(2)}, u32[]{:S(2)}) collective-permute-start(bf16[16,2176]{1,0:T(8,128)(2,1)S(1)} %mix.1.refs_0_.own_ref.packet_ref), channel_id=1, source_target_pairs={{0,24},{1,25},{2,26},{3,27},{4,28},{5,29},{6,30},{7,31},{8,16},{9,... | collective-permute-start | bytes 208904 | tf_op jit(solution)/shard_map/ppermute | solution.py:309
  25.4 2.3 %collective-permute-done.4.refs_3_ = bf16[16,2176]{1,0:T(8,128)(2,1)S(1)} collective-permute-done((bf16[16,2176]{1,0:T(8,128)(2,1)S(1)}, bf16[16,2176]{1,0:T(8,128)(2,1)S(1)}, u32[]{:S(2)}, u32[]{:S(2)}) %collective-permute-start.4) | collective-permute-done | bytes 69664 | tf_op jit(solution)/shard_map/ppermute | solution.py:309
  27.7 1.6 %collective-permute-start.11 = (bf16[64,2176]{1,0:T(8,128)(2,1)S(1)}, bf16[64,2176]{1,0:T(8,128)(2,1)S(1)}, u32[]{:S(2)}, u32[]{:S(2)}) collective-permute-start(bf16[64,2176]{1,0:T(8,128)(2,1)S(1)} %join.1.first_ref), channel_id=1, source_target_pairs={{0,4},{1,5},{2,6},{3,7},{4,0},{5,1},{6,2},{7,3},{8,12},{9,13},{10,... | collective-permute-start | bytes 835592 | tf_op jit(solution)/shard_map/ppermute | solution.py:309
  29.2 1.6 %collective-permute-done.9.refs_8_ = bf16[64,1024]{1,0:T(8,128)(2,1)S(1)} collective-permute-done((bf16[64,1024]{1,0:T(8,128)(2,1)}, bf16[64,1024]{1,0:T(8,128)(2,1)S(1)}, u32[]{:S(2)}, u32[]{:S(2)}) %collective-permute-start.9) | collective-permute-done | bytes 131104 | tf_op jit(solution)/shard_map/ppermute | solution.py:306
  31.4 1.4 %collective-permute-start.12 = (bf16[64,2176]{1,0:T(8,128)(2,1)S(1)}, bf16[64,2176]{1,0:T(8,128)(2,1)}, u32[]{:S(2)}, u32[]{:S(2)}) collective-permute-start(bf16[64,2176]{1,0:T(8,128)(2,1)S(1)} %join.1.first_ref), channel_id=1, source_target_pairs={{0,6},{1,7},{2,4},{3,5},{4,2},{5,3},{6,0},{7,1},{8,14},{9,15},{10,... | collective-permute-start | bytes 835592 | tf_op jit(solution)/shard_map/ppermute | solution.py:309
  32.9 1.4 %collective-permute-done.11.first_ref = bf16[64,2176]{1,0:T(8,128)(2,1)S(1)} collective-permute-done((bf16[64,2176]{1,0:T(8,128)(2,1)S(1)}, bf16[64,2176]{1,0:T(8,128)(2,1)S(1)}, u32[]{:S(2)}, u32[]{:S(2)}) %collective-permute-start.11) | collective-permute-done | bytes 278560 | tf_op jit(solution)/shard_map/ppermute | solution.py:309
  35.0 1.5 %collective-permute-start.5 = (bf16[64,2176]{1,0:T(8,128)(2,1)S(1)}, bf16[64,2176]{1,0:T(8,128)(2,1)}, u32[]{:S(2)}, u32[]{:S(2)}) collective-permute-start(bf16[64,2176]{1,0:T(8,128)(2,1)S(1)} %join.1.first_ref), channel_id=1, source_target_pairs={{0,2},{1,3},{2,0},{3,1},{4,6},{5,7},{6,4},{7,5},{8,10},{9,11},{10,... | collective-permute-start | bytes 835592 | tf_op jit(solution)/shard_map/ppermute | solution.py:309
  36.6 5.4 %collective-permute-done.12.second_ref = bf16[64,2176]{1,0:T(8,128)(2,1)} collective-permute-done((bf16[64,2176]{1,0:T(8,128)(2,1)S(1)}, bf16[64,2176]{1,0:T(8,128)(2,1)}, u32[]{:S(2)}, u32[]{:S(2)}) %collective-permute-start.12) | collective-permute-done | bytes 278560 | tf_op jit(solution)/shard_map/ppermute | solution.py:309
  42.0 1.2 %copy-done.3 = bf16[1,256,2048]{2,1,0:T(8,128)(2,1)S(1)} copy-done((bf16[1,256,2048]{2,1,0:T(8,128)(2,1)S(1)}, bf16[1,256,2048]{2,1,0:T(8,128)(2,1)}, u32[]{:S(2)}) %copy-start.3) | copy-done | bytes 1048600
  46.0 1.0 %copy-done.19 = bf16[64,2176]{1,0:T(8,128)(2,1)S(1)} copy-done((bf16[64,2176]{1,0:T(8,128)(2,1)S(1)}, bf16[64,2176]{1,0:T(8,128)(2,1)}, u32[]{:S(2)}) %copy-start.19) | copy-done | bytes 278552
  47.0 4.5 %routed_rows.3 = (bf16[64,2048]{1,0:T(8,128)(2,1)S(1)}, bf16[64,2048]{1,0:T(8,128)(2,1)S(1)}) custom-call(s32[2]{0:T(128)S(1)} %pad_add_fusion.place_ref, bf16[64,2176]{1,0:T(8,128)(2,1)S(1)} %copy-done.19, bf16[64,2176]{1,0:T(8,128)(2,1)} %collective-permute-done.12.second_ref, bf16[1,2048]{1,0:T(2,128)(2,1)S(1)} %broadcast_in_dim.11.branch_ref, ...), custom_call_target="tpu_custom_call" | custom-call | flops 805306368 | bytes 8388608 | tf_op jit(solution)/shard_map/routed_rows/pallas_call | solution.py:252
  51.5 1.5 %collective-permute-start.13 = (bf16[64,2048]{1,0:T(8,128)(2,1)S(1)}, bf16[64,2048]{1,0:T(8,128)(2,1)S(1)}, u32[]{:S(2)}, u32[]{:S(2)}) collective-permute-start(bf16[64,2048]{1,0:T(8,128)(2,1)S(1)} %get-tuple-element.16), channel_id=1, source_target_pairs={{4,0},{5,1},{6,2},{7,3},{0,4},{1,5},{2,6},{3,7},{12,8},{13,9},{14,... | collective-permute-start | bytes 786440 | tf_op jit(solution)/shard_map/ppermute | solution.py:309
  53.0 1.5 %collective-permute-start.14 = (bf16[64,2048]{1,0:T(8,128)(2,1)S(1)}, bf16[64,2048]{1,0:T(8,128)(2,1)S(1)}, u32[]{:S(2)}, u32[]{:S(2)}) collective-permute-start(bf16[64,2048]{1,0:T(8,128)(2,1)S(1)} %get-tuple-element.17), channel_id=1, source_target_pairs={{6,0},{7,1},{4,2},{5,3},{2,4},{3,5},{0,6},{1,7},{14,8},{15,9},{12,... | collective-permute-start | bytes 786440 | tf_op jit(solution)/shard_map/ppermute | solution.py:309
  54.5 4.4 %routed_rows.2 = (bf16[64,2048]{1,0:T(8,128)(2,1)S(1)}, bf16[64,2048]{1,0:T(8,128)(2,1)S(1)}) custom-call(s32[2]{0:T(128)S(1)} %pad_add_fusion.place_ref, bf16[64,2176]{1,0:T(8,128)(2,1)S(1)} %join.1.first_ref, bf16[64,2176]{1,0:T(8,128)(2,1)} %collective-permute-done.5.second_ref, bf16[1,2048]{1,0:T(2,128)(2,1)S(1)} %broadcast_in_dim.11.branch_ref, ...), custom_call_target="tpu_custom_call" | custom-call | flops 805306368 | bytes 8388608 | tf_op jit(solution)/shard_map/routed_rows/pallas_call | solution.py:252
  59.5 1.3 %collective-permute-done.18.far_ref = bf16[16,2176]{1,0:T(8,128)(2,1)S(1)} collective-permute-done((bf16[16,2176]{1,0:T(8,128)(2,1)S(1)}, bf16[16,2176]{1,0:T(8,128)(2,1)S(1)}, u32[]{:S(2)}, u32[]{:S(2)}) %collective-permute-start.18) | collective-permute-done | bytes 69664 | tf_op jit(solution)/shard_map/ppermute | solution.py:306
  60.8 1.3 %shared_mlp.1 = (bf16[16,2048]{1,0:T(8,128)(2,1)S(1)}, bf16[16,2048]{1,0:T(8,128)(2,1)S(1)}) custom-call(bf16[16,2176]{1,0:T(8,128)(2,1)S(1)} %mix.1.refs_0_.own_ref.packet_ref, bf16[16,2176]{1,0:T(8,128)(2,1)S(1)} %collective-permute-done.18.far_ref, bf16[2048,256]{1,0:T(8,128)(2,1)S(1)} %copy-done.6, bf16[2048,256]{1,0:T(8,128)(2,1)S(1)} %copy-done.7, ...), custom_call_target="tpu_custom_call" | custom-call | flops 100663296 | bytes 3145728 | tf_op jit(solution)/shard_map/shared_mlp/pallas_call | solution.py:370
  62.4 1.5 %collective-permute-done.13.refs_2_ = bf16[64,2048]{1,0:T(8,128)(2,1)S(1)} collective-permute-done((bf16[64,2048]{1,0:T(8,128)(2,1)S(1)}, bf16[64,2048]{1,0:T(8,128)(2,1)S(1)}, u32[]{:S(2)}, u32[]{:S(2)}) %collective-permute-start.13) | collective-permute-done | bytes 262176 | tf_op jit(solution)/shard_map/ppermute | solution.py:309
  63.8 1.5 %collective-permute-done.10.refs_1_ = bf16[64,2048]{1,0:T(8,128)(2,1)S(1)} collective-permute-done((bf16[64,2048]{1,0:T(8,128)(2,1)S(1)}, bf16[64,2048]{1,0:T(8,128)(2,1)S(1)}, u32[]{:S(2)}, u32[]{:S(2)}) %collective-permute-start.10) | collective-permute-done | bytes 262176 | tf_op jit(solution)/shard_map/ppermute | solution.py:309
  65.5 2.0 %collective-permute-start.15 = (bf16[16,2048]{1,0:T(8,128)(2,1)S(1)}, bf16[16,2048]{1,0:T(8,128)(2,1)S(1)}, u32[]{:S(2)}, u32[]{:S(2)}) collective-permute-start(bf16[16,2048]{1,0:T(8,128)(2,1)S(1)} %get-tuple-element.19), channel_id=1, source_target_pairs={{8,0},{9,1},{10,2},{11,3},{12,4},{13,5},{14,6},{15,7},{0,8},{1,9},... | collective-permute-start | bytes 196616 | tf_op jit(solution)/shard_map/ppermute | solution.py:309
  67.5 2.4 %collective-permute-start.16 = (bf16[16,2048]{1,0:T(8,128)(2,1)S(1)}, bf16[16,2048]{1,0:T(8,128)(2,1)S(1)}, u32[]{:S(2)}, u32[]{:S(2)}) collective-permute-start(bf16[16,2048]{1,0:T(8,128)(2,1)S(1)} %get-tuple-element.20), channel_id=1, source_target_pairs={{16,0},{17,1},{18,2},{19,3},{20,4},{21,5},{22,6},{23,7},{24,8},{25... | collective-permute-start | bytes 196616 | tf_op jit(solution)/shard_map/ppermute | solution.py:309
  70.1 1.2 %collective-permute-done.1.far_norm_ref = f32[2,1024]{1,0:T(2,128)S(1)} collective-permute-done((f32[2,1024]{1,0:T(2,128)S(1)}, f32[2,1024]{1,0:T(2,128)S(1)}, u32[]{:S(2)}, u32[]{:S(2)}) %collective-permute-start.1) | collective-permute-done | bytes 8224 | tf_op jit(solution)/shard_map/ppermute | solution.py:306
  71.2 2.4 %collective-permute-done.16.refs_2_ = bf16[16,2048]{1,0:T(8,128)(2,1)S(1)} collective-permute-done((bf16[16,2048]{1,0:T(8,128)(2,1)S(1)}, bf16[16,2048]{1,0:T(8,128)(2,1)S(1)}, u32[]{:S(2)}, u32[]{:S(2)}) %collective-permute-start.16) | collective-permute-done | bytes 65568 | tf_op jit(solution)/shard_map/ppermute | solution.py:309
  73.7 2.4 %collective-permute-done.17.refs_3_ = bf16[16,2048]{1,0:T(8,128)(2,1)S(1)} collective-permute-done((bf16[16,2048]{1,0:T(8,128)(2,1)S(1)}, bf16[16,2048]{1,0:T(8,128)(2,1)S(1)}, u32[]{:S(2)}, u32[]{:S(2)}) %collective-permute-start.17) | collective-permute-done | bytes 65568 | tf_op jit(solution)/shard_map/ppermute | solution.py:309
  76.4 1.1 %copy.47 = f32[2,32,16,64]{3,2,1,0:T(8,128)} copy(f32[2,32,16,64]{3,1,2,0:T(8,128)S(1)} %pad_maximum_fusion) | data formatting | bytes 524288
  (109 shorter events, 12.5 us)
Async XLA Ops:
  0.7 41.3 %collective-permute-start.6 = (bf16[1,2048,256]{2,1,0:T(8,128)(2,1)}, bf16[1,2048,256]{2,1,0:T(8,128)(2,1)}, u32[]{:S(2)}, u32[]{:S(2)}) collective-permute-start(bf16[1,2048,256]{2,1,0:T(8,128)(2,1)} %refs_0_.3), channel_id=1, source_target_pairs={{0,1},{1,0},{2,3},{3,2},{4,5},{5,4},{6,7},{7,6},{8,9},{9,8},{10,11... | collective-permute-start | bytes 3145736 | tf_op jit(solution)/shard_map/ppermute | solution.py:306
  1.2 40.7 %collective-permute-start.7 = (bf16[1,2048,256]{2,1,0:T(8,128)(2,1)}, bf16[1,2048,256]{2,1,0:T(8,128)(2,1)}, u32[]{:S(2)}, u32[]{:S(2)}) collective-permute-start(bf16[1,2048,256]{2,1,0:T(8,128)(2,1)} %refs_1_.3), channel_id=1, source_target_pairs={{0,1},{1,0},{2,3},{3,2},{4,5},{5,4},{6,7},{7,6},{8,9},{9,8},{10,11... | collective-permute-start | bytes 3145736 | tf_op jit(solution)/shard_map/ppermute | solution.py:306
  1.3 40.7 %collective-permute-start.8 = (bf16[1,256,2048]{2,1,0:T(8,128)(2,1)}, bf16[1,256,2048]{2,1,0:T(8,128)(2,1)}, u32[]{:S(2)}, u32[]{:S(2)}) collective-permute-start(bf16[1,256,2048]{2,1,0:T(8,128)(2,1)} %refs_4_.3), channel_id=1, source_target_pairs={{0,1},{1,0},{2,3},{3,2},{4,5},{5,4},{6,7},{7,6},{8,9},{9,8},{10,11... | collective-permute-start | bytes 3145736 | tf_op jit(solution)/shard_map/ppermute | solution.py:306
  6.6 29.8 %copy-start.33 = (bf16[2048]{0:T(1024)(128)(2,1)S(1)}, bf16[2048]{0:T(1024)(128)(2,1)}, u32[]{:S(2)}) copy-start(bf16[2048]{0:T(1024)(128)(2,1)} %param.49) | copy-start | bytes 12292
  7.2 34.8 %copy-start.1 = (bf16[1,2048,256]{2,1,0:T(8,128)(2,1)S(1)}, bf16[1,2048,256]{2,1,0:T(8,128)(2,1)}, u32[]{:S(2)}) copy-start(bf16[1,2048,256]{2,1,0:T(8,128)(2,1)} %refs_0_.3) | copy-start | bytes 3145732
  7.2 34.8 %copy-start.2 = (bf16[1,2048,256]{2,1,0:T(8,128)(2,1)S(1)}, bf16[1,2048,256]{2,1,0:T(8,128)(2,1)}, u32[]{:S(2)}) copy-start(bf16[1,2048,256]{2,1,0:T(8,128)(2,1)} %refs_1_.3) | copy-start | bytes 3145732
  10.5 1.2 %collective-permute-start = (bf16[16,256]{1,0:T(8,128)(2,1)S(1)}, bf16[16,256]{1,0:T(8,128)(2,1)S(1)}, u32[]{:S(2)}, u32[]{:S(2)}) collective-permute-start(bf16[16,256]{1,0:T(8,128)(2,1)S(1)} %constant_dynamic-slice_fusion), channel_id=1, source_target_pairs={{0,1},{1,0},{2,3},{3,2},{4,5},{5,4},{6,7},{7,6},{8,9},{9,8},{10,11... | collective-permute-start | bytes 24584 | tf_op jit(solution)/shard_map/ppermute | solution.py:306
  15.1 5.5 %collective-permute-start.2 = (bf16[16,2176]{1,0:T(8,128)(2,1)S(1)}, bf16[16,2176]{1,0:T(8,128)(2,1)S(1)}, u32[]{:S(2)}, u32[]{:S(2)}) collective-permute-start(bf16[16,2176]{1,0:T(8,128)(2,1)S(1)} %mix.1.refs_0_.own_ref.packet_ref), channel_id=1, source_target_pairs={{0,8},{1,9},{2,10},{3,11},{4,12},{5,13},{6,14},{7,15},{8,0},{9,1},... | collective-permute-start | bytes 208904 | tf_op jit(solution)/shard_map/ppermute | solution.py:309
  17.9 7.4 %collective-permute-start.3 = (bf16[16,2176]{1,0:T(8,128)(2,1)S(1)}, bf16[16,2176]{1,0:T(8,128)(2,1)S(1)}, u32[]{:S(2)}, u32[]{:S(2)}) collective-permute-start(bf16[16,2176]{1,0:T(8,128)(2,1)S(1)} %mix.1.refs_0_.own_ref.packet_ref), channel_id=1, source_target_pairs={{0,16},{1,17},{2,18},{3,19},{4,20},{5,21},{6,22},{7,23},{8,24},{9,... | collective-permute-start | bytes 208904 | tf_op jit(solution)/shard_map/ppermute | solution.py:309
  20.6 7.0 %collective-permute-start.4 = (bf16[16,2176]{1,0:T(8,128)(2,1)S(1)}, bf16[16,2176]{1,0:T(8,128)(2,1)S(1)}, u32[]{:S(2)}, u32[]{:S(2)}) collective-permute-start(bf16[16,2176]{1,0:T(8,128)(2,1)S(1)} %mix.1.refs_0_.own_ref.packet_ref), channel_id=1, source_target_pairs={{0,24},{1,25},{2,26},{3,27},{4,28},{5,29},{6,30},{7,31},{8,16},{9,... | collective-permute-start | bytes 208904 | tf_op jit(solution)/shard_map/ppermute | solution.py:309
  27.7 6.6 %collective-permute-start.11 = (bf16[64,2176]{1,0:T(8,128)(2,1)S(1)}, bf16[64,2176]{1,0:T(8,128)(2,1)S(1)}, u32[]{:S(2)}, u32[]{:S(2)}) collective-permute-start(bf16[64,2176]{1,0:T(8,128)(2,1)S(1)} %join.1.first_ref), channel_id=1, source_target_pairs={{0,4},{1,5},{2,6},{3,7},{4,0},{5,1},{6,2},{7,3},{8,12},{9,13},{10,... | collective-permute-start | bytes 835592 | tf_op jit(solution)/shard_map/ppermute | solution.py:309
  29.2 1.6 %collective-permute-start.9 = (bf16[64,1024]{1,0:T(8,128)(2,1)}, bf16[64,1024]{1,0:T(8,128)(2,1)S(1)}, u32[]{:S(2)}, u32[]{:S(2)}) collective-permute-start(bf16[64,1024]{1,0:T(8,128)(2,1)} %refs_7_.3), channel_id=1, source_target_pairs={{0,1},{1,0},{2,3},{3,2},{4,5},{5,4},{6,7},{7,6},{8,9},{9,8},{10,11... | collective-permute-start | bytes 393224 | tf_op jit(solution)/shard_map/ppermute | solution.py:306
  31.4 10.5 %collective-permute-start.12 = (bf16[64,2176]{1,0:T(8,128)(2,1)S(1)}, bf16[64,2176]{1,0:T(8,128)(2,1)}, u32[]{:S(2)}, u32[]{:S(2)}) collective-permute-start(bf16[64,2176]{1,0:T(8,128)(2,1)S(1)} %join.1.first_ref), channel_id=1, source_target_pairs={{0,6},{1,7},{2,4},{3,5},{4,2},{5,3},{6,0},{7,1},{8,14},{9,15},{10,... | collective-permute-start | bytes 835592 | tf_op jit(solution)/shard_map/ppermute | solution.py:309
  35.0 19.5 %collective-permute-start.5 = (bf16[64,2176]{1,0:T(8,128)(2,1)S(1)}, bf16[64,2176]{1,0:T(8,128)(2,1)}, u32[]{:S(2)}, u32[]{:S(2)}) collective-permute-start(bf16[64,2176]{1,0:T(8,128)(2,1)S(1)} %join.1.first_ref), channel_id=1, source_target_pairs={{0,2},{1,3},{2,0},{3,1},{4,6},{5,7},{6,4},{7,5},{8,10},{9,11},{10,... | collective-permute-start | bytes 835592 | tf_op jit(solution)/shard_map/ppermute | solution.py:309
  47.0 7.5 %copy-start.15 = (bf16[64,1024]{1,0:T(8,128)(2,1)S(1)}, bf16[64,1024]{1,0:T(8,128)(2,1)}, u32[]{:S(2)}) copy-start(bf16[64,1024]{1,0:T(8,128)(2,1)} %copy-done.13) | copy-start | bytes 393220
  51.5 12.4 %collective-permute-start.13 = (bf16[64,2048]{1,0:T(8,128)(2,1)S(1)}, bf16[64,2048]{1,0:T(8,128)(2,1)S(1)}, u32[]{:S(2)}, u32[]{:S(2)}) collective-permute-start(bf16[64,2048]{1,0:T(8,128)(2,1)S(1)} %get-tuple-element.16), channel_id=1, source_target_pairs={{4,0},{5,1},{6,2},{7,3},{0,4},{1,5},{2,6},{3,7},{12,8},{13,9},{14,... | collective-permute-start | bytes 786440 | tf_op jit(solution)/shard_map/ppermute | solution.py:309
  52.9 7.9 %copy-start.6 = (bf16[2048,256]{1,0:T(8,128)(2,1)S(1)}, bf16[2048,256]{1,0:T(8,128)(2,1)}, u32[]{:S(2)}) copy-start(bf16[2048,256]{1,0:T(8,128)(2,1)} %gate_hbm.1) | copy-start | bytes 3145732
  52.9 7.9 %copy-start.7 = (bf16[2048,256]{1,0:T(8,128)(2,1)S(1)}, bf16[2048,256]{1,0:T(8,128)(2,1)}, u32[]{:S(2)}) copy-start(bf16[2048,256]{1,0:T(8,128)(2,1)} %up_hbm.1) | copy-start | bytes 3145732
  52.9 7.9 %copy-start.8 = (bf16[256,2048]{1,0:T(8,128)(2,1)S(1)}, bf16[256,2048]{1,0:T(8,128)(2,1)}, u32[]{:S(2)}) copy-start(bf16[256,2048]{1,0:T(8,128)(2,1)} %down_hbm.1) | copy-start | bytes 3145732
  53.0 10.9 %collective-permute-start.14 = (bf16[64,2048]{1,0:T(8,128)(2,1)S(1)}, bf16[64,2048]{1,0:T(8,128)(2,1)S(1)}, u32[]{:S(2)}, u32[]{:S(2)}) collective-permute-start(bf16[64,2048]{1,0:T(8,128)(2,1)S(1)} %get-tuple-element.17), channel_id=1, source_target_pairs={{6,0},{7,1},{4,2},{5,3},{2,4},{3,5},{0,6},{1,7},{14,8},{15,9},{12,... | collective-permute-start | bytes 786440 | tf_op jit(solution)/shard_map/ppermute | solution.py:309
  58.9 11.1 %copy-start.34 = (f32[1024]{0:T(1024)S(1)}, f32[1024]{0:T(1024)}, u32[]{:S(2)}) copy-start(f32[1024]{0:T(1024)} %param.51) | copy-start | bytes 12292
  58.9 11.1 %copy-start.35 = (f32[1024]{0:T(1024)S(1)}, f32[1024]{0:T(1024)}, u32[]{:S(2)}) copy-start(f32[1024]{0:T(1024)} %param.50) | copy-start | bytes 12292
  58.9 17.4 %copy-start.23 = (f32[32,16,64]{2,0,1:T(8,128)S(1)}, f32[32,16,64]{2,0,1:T(8,128)}, u32[]{:S(2)}) copy-start(f32[32,16,64]{2,0,1:T(8,128)} %copy-done.22) | copy-start | bytes 393220
  58.9 17.4 %copy-start.25 = (f32[32,16,64]{2,0,1:T(8,128)S(1)}, f32[32,16,64]{2,0,1:T(8,128)}, u32[]{:S(2)}) copy-start(f32[32,16,64]{2,0,1:T(8,128)} %copy-done.24) | copy-start | bytes 393220
  58.9 6.4 %collective-permute-start.10 = (bf16[64,2048]{1,0:T(8,128)(2,1)S(1)}, bf16[64,2048]{1,0:T(8,128)(2,1)S(1)}, u32[]{:S(2)}, u32[]{:S(2)}) collective-permute-start(bf16[64,2048]{1,0:T(8,128)(2,1)S(1)} %get-tuple-element.15), channel_id=1, source_target_pairs={{2,0},{3,1},{0,2},{1,3},{6,4},{7,5},{4,6},{5,7},{10,8},{11,9},{8,1... | collective-permute-start | bytes 786440 | tf_op jit(solution)/shard_map/ppermute | solution.py:309
  59.5 1.3 %collective-permute-start.18 = (bf16[16,2176]{1,0:T(8,128)(2,1)S(1)}, bf16[16,2176]{1,0:T(8,128)(2,1)S(1)}, u32[]{:S(2)}, u32[]{:S(2)}) collective-permute-start(bf16[16,2176]{1,0:T(8,128)(2,1)S(1)} %mix.1.refs_0_.own_ref.packet_ref), channel_id=1, source_target_pairs={{0,1},{1,0},{2,3},{3,2},{4,5},{5,4},{6,7},{7,6},{8,9},{9,8},{10,11... | collective-permute-start | bytes 208904 | tf_op jit(solution)/shard_map/ppermute | solution.py:306
  62.1 9.1 %collective-permute-start.19 = (bf16[16,2048]{1,0:T(8,128)(2,1)S(1)}, bf16[16,2048]{1,0:T(8,128)(2,1)S(1)}, u32[]{:S(2)}, u32[]{:S(2)}) collective-permute-start(bf16[16,2048]{1,0:T(8,128)(2,1)S(1)} %get-tuple-element.23), channel_id=1, source_target_pairs={{0,1},{1,0},{2,3},{3,2},{4,5},{5,4},{6,7},{7,6},{8,9},{9,8},{10,11... | collective-permute-start | bytes 196616 | tf_op jit(solution)/shard_map/ppermute | solution.py:306
  65.5 5.7 %collective-permute-start.15 = (bf16[16,2048]{1,0:T(8,128)(2,1)S(1)}, bf16[16,2048]{1,0:T(8,128)(2,1)S(1)}, u32[]{:S(2)}, u32[]{:S(2)}) collective-permute-start(bf16[16,2048]{1,0:T(8,128)(2,1)S(1)} %get-tuple-element.19), channel_id=1, source_target_pairs={{8,0},{9,1},{10,2},{11,3},{12,4},{13,5},{14,6},{15,7},{0,8},{1,9},... | collective-permute-start | bytes 196616 | tf_op jit(solution)/shard_map/ppermute | solution.py:309
  67.5 6.2 %collective-permute-start.16 = (bf16[16,2048]{1,0:T(8,128)(2,1)S(1)}, bf16[16,2048]{1,0:T(8,128)(2,1)S(1)}, u32[]{:S(2)}, u32[]{:S(2)}) collective-permute-start(bf16[16,2048]{1,0:T(8,128)(2,1)S(1)} %get-tuple-element.20), channel_id=1, source_target_pairs={{16,0},{17,1},{18,2},{19,3},{20,4},{21,5},{22,6},{23,7},{24,8},{25... | collective-permute-start | bytes 196616 | tf_op jit(solution)/shard_map/ppermute | solution.py:309
  70.0 6.1 %collective-permute-start.17 = (bf16[16,2048]{1,0:T(8,128)(2,1)S(1)}, bf16[16,2048]{1,0:T(8,128)(2,1)S(1)}, u32[]{:S(2)}, u32[]{:S(2)}) collective-permute-start(bf16[16,2048]{1,0:T(8,128)(2,1)S(1)} %get-tuple-element.21), channel_id=1, source_target_pairs={{24,0},{25,1},{26,2},{27,3},{28,4},{29,5},{30,6},{31,7},{16,8},{17... | collective-permute-start | bytes 196616 | tf_op jit(solution)/shard_map/ppermute | solution.py:309
  70.0 1.2 %collective-permute-start.1 = (f32[2,1024]{1,0:T(2,128)S(1)}, f32[2,1024]{1,0:T(2,128)S(1)}, u32[]{:S(2)}, u32[]{:S(2)}) collective-permute-start(f32[2,1024]{1,0:T(2,128)S(1)} %pad_maximum_fusion.1.own_norm_ref), channel_id=1, source_target_pairs={{0,1},{1,0},{2,3},{3,2},{4,5},{5,4},{6,7},{7,6},{8,9},{9,8},{10,11... | collective-permute-start | bytes 24584 | tf_op jit(solution)/shard_map/ppermute | solution.py:306
  76.2 1.3 %collective-permute-start.20 = (bf16[16,1024]{1,0:T(8,128)(2,1)S(1)}, bf16[16,1024]{1,0:T(8,128)(2,1)S(1)}, u32[]{:S(2)}, u32[]{:S(2)}) collective-permute-start(bf16[16,1024]{1,0:T(8,128)(2,1)S(1)} %get-tuple-element.25), channel_id=1, source_target_pairs={{0,1},{1,0},{2,3},{3,2},{4,5},{5,4},{6,7},{7,6},{8,9},{9,8},{10,11... | collective-permute-start | bytes 98312 | tf_op jit(solution)/shard_map/ppermute | solution.py:306
  (25 other events, 90.4 us)

commit v2 on v1

--- a/solution.py
+++ b/solution.py
@@ -11,34 +11,7 @@
 residual_alpha = 1.681792830507429
 route_scale = 2.5
 norm_eps = 1e-05
-highest = lax.Precision.HIGHEST
 both_axes = ("ep", "tp")
-
-
-def state_update(
-    inputs, ssm_state, decay_rate, frequency, step_log, input_map, output_map, skip_gain
-):
-    step_size = jnp.exp(step_log)[:, None]
-    magnitude = jnp.exp(-decay_rate * step_size)
-    rotation = frequency * step_size
-    decay_re = magnitude * jnp.cos(rotation)
-    decay_im = magnitude * jnp.sin(rotation)
-    eigen_re = -decay_rate
-    denominator = eigen_re * eigen_re + frequency * frequency
-    factor_re = ((decay_re - 1.0) * eigen_re + decay_im * frequency) / denominator
-    factor_im = (decay_im * eigen_re - (decay_re - 1.0) * frequency) / denominator
-    drive_re = factor_re[..., None] * input_map[0] - factor_im[..., None] * input_map[1]
-    drive_im = factor_re[..., None] * input_map[1] + factor_im[..., None] * input_map[0]
-    pushed_re = jnp.einsum("gpm,tgm->tgp", drive_re, inputs, precision=highest)
-    pushed_im = jnp.einsum("gpm,tgm->tgp", drive_im, inputs, precision=highest)
-    new_re = decay_re * ssm_state[0] - decay_im * ssm_state[1] + pushed_re
-    new_im = decay_re * ssm_state[1] + decay_im * ssm_state[0] + pushed_im
-    response = (
-        jnp.einsum("gmp,tgp->tgm", output_map[0], new_re, precision=highest)
-        - jnp.einsum("gmp,tgp->tgm", output_map[1], new_im, precision=highest)
-        + skip_gain * inputs
-    )
-    return (response, jnp.stack([new_re, new_im]))
 
 
 def split_of(count_ep):
@@ -74,7 +47,7 @@
 
 vmem = pl.BlockSpec(memory_space=pltpu.VMEM)
 smem = pl.BlockSpec(memory_space=pltpu.SMEM)
-anywhere = pl.BlockSpec(memory_space=pl.ANY)
+in_hbm = pl.BlockSpec(memory_space=pltpu.HBM)
 
 
 def product(left, right):
@@ -92,6 +65,94 @@
 def token_half(ref, flipped):
     half = ref.shape[0] // 2
     return jnp.where(flipped, ref[half:, :], ref[:half, :])
+
+
+def halves(value):
+    high = value.astype(jnp.bfloat16)
+    return high, (value - high.astype(jnp.float32)).astype(jnp.bfloat16)
+
+
+def mixer_kernel(core_ref, *refs):
+    sources, (own_ref, far_ref, new_ref) = refs[:9], refs[9:12]
+    held, sems = refs[12:21], refs[21]
+    copies = []
+    for index, (source, target) in enumerate(zip(sources, held)):
+        copies.append(pltpu.make_async_copy(source, target, sems.at[index]))
+        copies[-1].start()
+    step_ref, rate_ref, frequency_ref, input_ref, project_ref, drive_ref, state_ref, readout_ref, skip_ref = held
+    rows = input_ref.shape[0]
+    groups, _ = rate_ref.shape
+    channels = skip_ref.shape[1]
+    for copy in copies[:3]:
+        copy.wait()
+    square = lax.broadcasted_iota(jnp.int32, (groups, groups), 0) == lax.broadcasted_iota(
+        jnp.int32, (groups, groups), 1
+    )
+    step_size = jnp.exp(jnp.sum(jnp.where(square, step_ref[...], 0.0), axis=1, keepdims=True))
+    rate, frequency = rate_ref[...], frequency_ref[...]
+    magnitude = jnp.exp(-rate * step_size)
+    rotation = frequency * step_size
+    decay_re = magnitude * jnp.cos(rotation)
+    decay_im = magnitude * jnp.sin(rotation)
+    denominator = rate * rate + frequency * frequency
+    factor_re = (decay_im * frequency - (decay_re - 1.0) * rate) / denominator
+    factor_im = (-decay_im * rate - (decay_re - 1.0) * frequency) / denominator
+    for copy in copies[3:]:
+        copy.wait()
+    flipped = core_ref[0] == 1
+    projected = product(input_ref[...], project_ref[...]).astype(jnp.bfloat16)
+    responses = []
+    for index in range(groups):
+        one = slice(index, index + 1)
+        inputs = projected[:, index * channels : (index + 1) * channels]
+        twice = jnp.concatenate([inputs, inputs], axis=1)
+        map_re, map_im = drive_ref[0, index], drive_ref[1, index]
+        drive_re = halves(factor_re[one] * map_re - factor_im[one] * map_im)
+        drive_im = halves(factor_re[one] * map_im + factor_im[one] * map_re)
+        old_re = state_ref[pl.ds(index, rows, groups), :]
+        old_im = state_ref[pl.ds(rows * groups + index, rows, groups), :]
+        new_re = decay_re[one] * old_re - decay_im[one] * old_im
+        new_im = decay_re[one] * old_im + decay_im[one] * old_re
+        new_re = new_re + product(twice, jnp.concatenate(drive_re, axis=0))
+        new_im = new_im + product(twice, jnp.concatenate(drive_im, axis=0))
+        new_ref[pl.ds(index, rows, groups), :] = new_re
+        new_ref[pl.ds(rows * groups + index, rows, groups), :] = new_im
+        high, low = halves(jnp.concatenate([new_re, new_im], axis=1))
+        readout = jnp.concatenate([readout_ref[0, index], -readout_ref[1, index]], axis=1)
+        read_high, read_low = halves(readout)
+        response = lax.dot_general(
+            jnp.concatenate([high, low, high], axis=1),
+            jnp.concatenate([read_high, read_high, read_low], axis=1),
+            (((1,), (1,)), ((), ())),
+            preferred_element_type=jnp.float32,
+        )
+        responses.append(response + skip_ref[one, :] * inputs.astype(jnp.float32))
+    activated = jax.nn.gelu(jnp.concatenate(responses, axis=1)).astype(jnp.bfloat16)
+    own_ref[...] = jnp.where(flipped, activated[rows // 2 :], activated[: rows // 2])
+    far_ref[...] = jnp.where(flipped, activated[: rows // 2], activated[rows // 2 :])
+
+
+def load_kernel(count, *refs):
+    sems = refs[2 * count]
+    copies = []
+    for index in range(count):
+        copies.append(pltpu.make_async_copy(refs[index], refs[count + index], sems.at[index]))
+        copies[-1].start()
+    for copy in copies:
+        copy.wait()
+
+
+def loaded(values):
+    return pl.pallas_call(
+        functools.partial(load_kernel, len(values)),
+        out_shape=[jax.ShapeDtypeStruct(value.shape, value.dtype) for value in values],
+        in_specs=[in_hbm] * len(values),
+        out_specs=[vmem] * len(values),
+        scratch_shapes=[pltpu.SemaphoreType.DMA((len(values),))],
+        compiler_params=params(12),
+        cost_estimate=cost(1 << 22, 8 << 20),
+        name="load",
+    )(*values)
 
 
 def mix_kernel(
@@ -110,7 +171,7 @@
 ):
     width = input_ref.shape[1]
     flipped = core_ref[0] == 1
-    own, far = token_half(own_ref, flipped), far_ref[...]
+    own, far = own_ref[...], far_ref[...]
     every = jnp.concatenate([jnp.where(flipped, far, own), jnp.where(flipped, own, far)], axis=1)
     gated = (every.astype(jnp.float32) * jax.nn.sigmoid(product(every, glu_ref[...]))).astype(
         jnp.bfloat16
@@ -195,14 +256,7 @@
 
 
 def routed_kernel(width, experts, local, place_ref, first_ref, second_ref, branch_ref, *refs):
-    weights, outs = refs[:9], refs[9:11]
-    held, sems = refs[11:20], refs[20]
-    copies = [
-        pltpu.make_async_copy(source, target, sems.at[index])
-        for index, (source, target) in enumerate(zip(weights, held))
-    ]
-    for copy in copies:
-        copy.start()
+    held, outs = refs[:9], refs[9:11]
     own_expert, core = place_ref[0], place_ref[1]
     rows = jnp.concatenate([first_ref[...], second_ref[...]], axis=0)
     block = first_ref.shape[0]
@@ -218,20 +272,15 @@
     )
     hidden = []
     for side in range(2):
-        copies[2 * side].wait()
-        copies[2 * side + 1].wait()
         for index in range(local):
             gate_part = product(tokens, held[2 * side][index])
             up_part = product(tokens, held[2 * side + 1][index])
             piece = jax.nn.silu(gate_part) * up_part * shares[index]
             hidden.append((piece.astype(jnp.bfloat16), held[4 + side], index))
-    copies[6].wait()
     dense_part = lax.dot_general(
         tokens, held[6][...], (((1,), (1,)), ((), ())), preferred_element_type=jnp.float32
     )
     dense_hidden = (jax.nn.gelu(dense_part) * jax.nn.sigmoid(logit)).astype(jnp.bfloat16)
-    for index in (4, 5, 7, 8):
-        copies[index].wait()
     part = width // 2
     for side in range(2):
         own_side = core == side
@@ -252,11 +301,9 @@
     return pl.pallas_call(
         functools.partial(routed_kernel, width, experts, weights[0].shape[0]),
         out_shape=[jax.ShapeDtypeStruct((rows, width), jnp.bfloat16)] * 2,
-        in_specs=[smem, vmem, vmem, vmem] + [anywhere] * len(weights),
+        in_specs=[smem, vmem, vmem, vmem] + [vmem] * len(weights),
         out_specs=[vmem] * 2,
-        scratch_shapes=[pltpu.VMEM(value.shape, value.dtype) for value in weights]
-        + [pltpu.SemaphoreType.DMA((len(weights),))],
-        compiler_params=params(28),
+        compiler_params=params(16),
         cost_estimate=cost(24 * rows * weights[0].size, 8 << 20),
         name="routed_rows",
     )(place, first, second, branch_gate[None, :], *weights)
@@ -296,7 +343,6 @@
     rank = lax.axis_index("ep")
     outer, inner = split_of(count_ep)
     seq_rows, width = layer_input.shape
-    local_groups, channels = skip_gain.shape
     local_experts = gate_expert.shape[0]
     experts = local_experts * count_ep
     place = jnp.stack([rank * local_experts, core]).astype(jnp.int32)
@@ -314,18 +360,36 @@
     down_far = swapped(down_expert)
     dense_far = swapped(dense_out)
     norm_far = swapped(norm_own)
-    projected = jnp.dot(layer_input, w_input, preferred_element_type=jnp.float32).astype(
-        jnp.bfloat16
-    )
-    inputs = projected.astype(jnp.float32).reshape(seq_rows, local_groups, channels)
-    response, new_state = state_update(
-        inputs, ssm_state, decay_rate, frequency, step_log, input_map, output_map, skip_gain
-    )
-    activated = jax.nn.gelu(response.reshape(seq_rows, local_groups * channels)).astype(
-        jnp.bfloat16
-    )
     core_rows = seq_rows // count_tp
-    far_tokens = lax.dynamic_slice_in_dim(activated, (1 - core) * core_rows, core_rows, 0)
+    state_rows = ssm_state.reshape(-1, ssm_state.shape[3])
+    half_channels = jax.ShapeDtypeStruct((core_rows, w_input.shape[1]), jnp.bfloat16)
+    sources = [
+        step_log[None, :],
+        decay_rate,
+        frequency,
+        layer_input,
+        w_input,
+        jnp.swapaxes(input_map, 2, 3),
+        state_rows,
+        output_map,
+        skip_gain,
+    ]
+    activated, far_tokens, new_rows = pl.pallas_call(
+        mixer_kernel,
+        out_shape=[
+            half_channels,
+            half_channels,
+            jax.ShapeDtypeStruct(state_rows.shape, jnp.float32),
+        ],
+        in_specs=[smem] + [in_hbm] * len(sources),
+        out_specs=[vmem] * 3,
+        scratch_shapes=[pltpu.VMEM(value.shape, value.dtype) for value in sources]
+        + [pltpu.SemaphoreType.DMA((len(sources),))],
+        compiler_params=params(63),
+        cost_estimate=cost(4 * seq_rows * w_input.size, 5 << 20),
+        name="mixer",
+    )(core_word, *sources)
+    new_state = new_rows.reshape(ssm_state.shape)
     activated_far = swapped(far_tokens)
     packet_width = width + -(-2 * experts // 128) * 128
     packet_shape = jax.ShapeDtypeStruct((core_rows, packet_width), jnp.bfloat16)
@@ -366,11 +430,25 @@
     arrived = [line]
     for step in range(1, inner):
         arrived.append(moved(line, plane_moves(step, count_ep, count_tp)))
+    gate_held, up_held, down_held, dense_held = loaded([gate_far, up_far, down_far, dense_far])
+    weights = [gate_expert, up_expert, gate_held, up_held, down_expert, down_held]
+    weights += [dense_in, dense_out, dense_held]
+    results = {}
+    steps = [*range(1, inner), 0]
+    for slot in range(inner // 2):
+        pair = steps[2 * slot : 2 * slot + 2]
+        first, second = (arrived[step] for step in pair)
+        done = routed_rows(width, place, first, second, branch_gate, experts, weights)
+        results.update(zip(pair, done))
+    parts = [results[0]]
+    for step in range(1, inner):
+        moves = backward(plane_moves(step, count_ep, count_tp))
+        parts.append(moved(results[step], moves))
     held = (gate_shared, up_shared, down_shared)
     shared, shared_sent = pl.pallas_call(
         shared_kernel,
         out_shape=[row_shape] * 2,
-        in_specs=[vmem] * 2 + [anywhere] * 3,
+        in_specs=[vmem] * 2 + [in_hbm] * 3,
         out_specs=[vmem] * 2,
         scratch_shapes=[pltpu.VMEM(value.shape, value.dtype) for value in held]
         + [pltpu.SemaphoreType.DMA((3,))],
@@ -379,16 +457,6 @@
         name="shared_mlp",
     )(packet, packet_far, *held)
     shared_far = swapped(shared_sent)
-    weights = [gate_expert, up_expert, gate_far, up_far, down_expert, down_far]
-    weights += [dense_in, dense_out, dense_far]
-    results = []
-    for slot in range(inner // 2):
-        first, second = arrived[slot * 2 : slot * 2 + 2]
-        results += routed_rows(width, place, first, second, branch_gate, experts, weights)
-    parts = [results[0]]
-    for step in range(1, inner):
-        moves = backward(plane_moves(step, count_ep, count_tp))
-        parts.append(moved(results[step], moves))
     blocks = pl.pallas_call(
         functools.partial(sum_kernel, inner),
         out_shape=[row_shape] * outer,

time: 78.6 us -> 69.7 us (0.89)
  local copies, waits for them, and re-layouts: 13.9 us -> 4.1 us
  Pallas kernels: 11.9 us -> 17.1 us
  matrix products: 4.8 us -> 0 us
  waiting for transfers between devices: 21.9 us -> 25.8 us
  starting transfers between devices: 24.3 us -> 21.4 us
    pallas_call x0 -> x2, Pallas kernels: none -> 8.44 us  [the longest x1 6.54 us: body(): pl.pallas_call(mixer_kernel, out_shape=[half_channels, half_channels, jax...]
    unnamed x75 -> x42, local copies, waits for them, and re-layouts: 11 us -> 4.09 us
    dot_general x5 -> x0, matrix products: 4.8 us -> none  [the longest x1 2.24 us: state_update(): jnp.einsum('gmp,tgp->tgm', output_map[1], new_im, precision=highest)]
    ppermute x12, waiting for transfers between devices: 17 us -> 21 us  [moved(): return lax.ppermute(value, both_axes, moves)]
    pallas_call x2, Pallas kernels: 8.86 us -> 5.64 us  [routed_rows(): pl.pallas_call(functools.partial(routed_kernel, width, experts, weights[0...]
    ppermute x12, starting transfers between devices: 22.7 us -> 19.8 us  [moved(): return lax.ppermute(value, both_axes, moves)]
    slice x1 -> x0, local copies, waits for them, and re-layouts: 1.11 us -> none  [state_update(): new_re = decay_re * ssm_state[0] - decay_im * ssm_state[1] + pushed_re]
    reshape x1 -> x0, local copies, waits for them, and re-layouts: 0.97 us -> none  [body(): response.reshape(seq_rows, local_groups * channels)]
  transfers between devices with their start and end apart: 21 -> 21, of which waited for: 12 -> 12; matrix products, arithmetic and copies ran while one was open for 12% -> 0% of each run, Pallas kernels for 14% -> 24%
where the time goes in v2:
time: 69.7 us; the launch traced here: 69.4 us
  waiting for transfers between devices  25.8 us (37%)
  starting transfers between devices  21.4 us (31%)
  Pallas kernels  17.1 us (25%)
  local copies, waits for them, and re-layouts  4.1 us (6%)
  between operations  0.88 us (1%)
    ppermute x12, waiting for transfers between devices, moved(): return lax.ppermute(value, both_axes, moves)  21 us
    ppermute x12, starting transfers between devices, moved(): return lax.ppermute(value, both_axes, moves)  19.8 us
    pallas_call x1, Pallas kernels, body(): pl.pallas_call(mixer_kernel, out_shape=[half_channels, half_channels, jax...  6.54 us
    pallas_call x2, Pallas kernels, routed_rows(): pl.pallas_call(functools.partial(routed_kernel, width, experts, weights[0...  5.64 us
    ppermute x9, waiting for transfers between devices, swapped(): return lax.ppermute(value, 'tp', [(t, 1 - t) for t in range(count_tp)])  4.74 us
    unnamed x42, local copies, waits for them, and re-layouts  4.09 us
    pallas_call x1, Pallas kernels, loaded(): pl.pallas_call(functools.partial(load_kernel, len(values)), out_shape=[ja...  1.89 us
    ppermute x9, starting transfers between devices, swapped(): return lax.ppermute(value, 'tp', [(t, 1 - t) for t in range(count_tp)])  1.58 us
  transfers between devices with their start and end apart: 21, of which 12 were waited for; matrix products, arithmetic and copies ran while one was open for 0% of the time, Pallas kernels for 24%

profile of v2, /device:TPU:0, one launch (start us, length us, event | category | flops | bytes accessed | tf_op | source)
XLA Modules:
  0.0 69.4 jit_solution(9534113857910741500)
XLA Ops:
  1.8 6.5 %mixer.1 = (bf16[16,256]{1,0:T(8,128)(2,1)}, bf16[16,256]{1,0:T(8,128)(2,1)}, f32[1024,64]{1,0:T(8,128)}) custom-call(s32[1]{0:T(128)} %bitcast.core_ref, f32[1,16]{1,0:T(1,128)} %bitcast.16, f32[16,64]{1,0:T(8,128)} %refs_1_.3, f32[16,64]{1,0:T(8,128)} %refs_2_.1, bf16[32,2048]{1,0:T(8,128)(2,1)} %input_ref.1, bf16[2048,256]{1,0:T(8,128)(2,1)} %refs_4_.3, ...), custom_call_target="tpu_custom_call" | custom-call | flops 67108864 | bytes 5242880 | tf_op jit(solution)/shard_map/mixer/pallas_call | solution.py:377
  8.7 1.1 %collective-permute-done.far_ref = bf16[16,256]{1,0:T(8,128)(2,1)S(1)} collective-permute-done((bf16[16,256]{1,0:T(8,128)(2,1)}, bf16[16,256]{1,0:T(8,128)(2,1)S(1)}, u32[]{:S(2)}, u32[]{:S(2)}) %collective-permute-start) | collective-permute-done | bytes 8224 | tf_op jit(solution)/shard_map/ppermute | solution.py:352
  9.8 1.6 %copy-done.3 = bf16[512,2048]{1,0:T(8,128)(2,1)S(1)} copy-done((bf16[512,2048]{1,0:T(8,128)(2,1)S(1)}, bf16[512,2048]{1,0:T(8,128)(2,1)}, u32[]{:S(2)}) %copy-start.3) | copy-done | bytes 2097176
  11.4 0.7 %copy-done.14 = bf16[16,256]{1,0:T(8,128)(2,1)S(1)} copy-done((bf16[16,256]{1,0:T(8,128)(2,1)S(1)}, bf16[16,256]{1,0:T(8,128)(2,1)}, u32[]{:S(2)}) %copy-start.14) | copy-done | bytes 8216
  12.1 0.8 %mix.1.refs_0_.own_ref.packet_ref = bf16[16,2176]{1,0:T(8,128)(2,1)S(1)} custom-call(s32[1]{0:T(128)} %bitcast.core_ref, bf16[16,256]{1,0:T(8,128)(2,1)S(1)} %copy-done.14, bf16[16,256]{1,0:T(8,128)(2,1)S(1)} %collective-permute-done.far_ref, bf16[512,512]{1,0:T(8,128)(2,1)S(1)} %copy-done.8, bf16[512,2048]{1,0:T(8,128)(2,1)S(1)} %copy-done.3, ...), custom_call_target="tpu_custom_call" | custom-call | flops 83886080 | bytes 3145728 | tf_op jit(solution)/shard_map/mix/pallas_call | solution.py:397
  12.9 2.8 %collective-permute-start.2 = (bf16[16,2176]{1,0:T(8,128)(2,1)S(1)}, bf16[16,2176]{1,0:T(8,128)(2,1)S(1)}, u32[]{:S(2)}, u32[]{:S(2)}) collective-permute-start(bf16[16,2176]{1,0:T(8,128)(2,1)S(1)} %mix.1.refs_0_.own_ref.packet_ref), channel_id=1, source_target_pairs={{0,8},{1,9},{2,10},{3,11},{4,12},{5,13},{6,14},{7,15},{8,0},{9,1},... | collective-permute-start | bytes 208904 | tf_op jit(solution)/shard_map/ppermute | solution.py:355
  15.7 2.6 %collective-permute-start.3 = (bf16[16,2176]{1,0:T(8,128)(2,1)S(1)}, bf16[16,2176]{1,0:T(8,128)(2,1)S(1)}, u32[]{:S(2)}, u32[]{:S(2)}) collective-permute-start(bf16[16,2176]{1,0:T(8,128)(2,1)S(1)} %mix.1.refs_0_.own_ref.packet_ref), channel_id=1, source_target_pairs={{0,16},{1,17},{2,18},{3,19},{4,20},{5,21},{6,22},{7,23},{8,24},{9,... | collective-permute-start | bytes 208904 | tf_op jit(solution)/shard_map/ppermute | solution.py:355
  18.4 3.9 %collective-permute-done.3.refs_2_ = bf16[16,2176]{1,0:T(8,128)(2,1)S(1)} collective-permute-done((bf16[16,2176]{1,0:T(8,128)(2,1)S(1)}, bf16[16,2176]{1,0:T(8,128)(2,1)S(1)}, u32[]{:S(2)}, u32[]{:S(2)}) %collective-permute-start.3) | collective-permute-done | bytes 69664 | tf_op jit(solution)/shard_map/ppermute | solution.py:355
  22.3 2.6 %collective-permute-start.4 = (bf16[16,2176]{1,0:T(8,128)(2,1)S(1)}, bf16[16,2176]{1,0:T(8,128)(2,1)S(1)}, u32[]{:S(2)}, u32[]{:S(2)}) collective-permute-start(bf16[16,2176]{1,0:T(8,128)(2,1)S(1)} %mix.1.refs_0_.own_ref.packet_ref), channel_id=1, source_target_pairs={{0,24},{1,25},{2,26},{3,27},{4,28},{5,29},{6,30},{7,31},{8,16},{9,... | collective-permute-start | bytes 208904 | tf_op jit(solution)/shard_map/ppermute | solution.py:355
  24.9 3.5 %collective-permute-done.4.refs_3_ = bf16[16,2176]{1,0:T(8,128)(2,1)S(1)} collective-permute-done((bf16[16,2176]{1,0:T(8,128)(2,1)S(1)}, bf16[16,2176]{1,0:T(8,128)(2,1)S(1)}, u32[]{:S(2)}, u32[]{:S(2)}) %collective-permute-start.4) | collective-permute-done | bytes 69664 | tf_op jit(solution)/shard_map/ppermute | solution.py:355
  28.4 1.6 %collective-permute-start.10 = (bf16[64,2176]{1,0:T(8,128)(2,1)S(1)}, bf16[64,2176]{1,0:T(8,128)(2,1)}, u32[]{:S(2)}, u32[]{:S(2)}) collective-permute-start(bf16[64,2176]{1,0:T(8,128)(2,1)S(1)} %join.1.second_ref), channel_id=1, source_target_pairs={{0,2},{1,3},{2,0},{3,1},{4,6},{5,7},{6,4},{7,5},{8,10},{9,11},{10,... | collective-permute-start | bytes 835592 | tf_op jit(solution)/shard_map/ppermute | solution.py:355
  30.0 0.7 copy-done.10
  30.6 1.5 %collective-permute-start.11 = (bf16[64,2176]{1,0:T(8,128)(2,1)S(1)}, bf16[64,2176]{1,0:T(8,128)(2,1)}, u32[]{:S(2)}, u32[]{:S(2)}) collective-permute-start(bf16[64,2176]{1,0:T(8,128)(2,1)S(1)} %join.1.second_ref), channel_id=1, source_target_pairs={{0,4},{1,5},{2,6},{3,7},{4,0},{5,1},{6,2},{7,3},{8,12},{9,13},{10,... | collective-permute-start | bytes 835592 | tf_op jit(solution)/shard_map/ppermute | solution.py:355
  32.7 0.9 %copy-done.11 = bf16[64,1024]{1,0:T(8,128)(2,1)S(1)} copy-done((bf16[64,1024]{1,0:T(8,128)(2,1)S(1)}, bf16[64,1024]{1,0:T(8,128)(2,1)}, u32[]{:S(2)}) %copy-start.11) | copy-done | bytes 131096
  33.6 1.9 %load.1 = (bf16[1,2048,256]{2,1,0:T(8,128)(2,1)S(1)}, bf16[1,2048,256]{2,1,0:T(8,128)(2,1)S(1)}, bf16[1,256,2048]{2,1,0:T(8,128)(2,1)S(1)}, bf16[64,1024]{1,0:T(8,128)(2,1)S(1)}) custom-call(bf16[1,2048,256]{2,1,0:T(8,128)(2,1)} %collective-permute-done.6.refs_0_, bf16[1,2048,256]{2,1,0:T(8,128)(2,1)} %collective-permute-done.7.refs_1_, ...), custom_call_target="tpu_custom_call" | custom-call | flops 4194304 | bytes 8388608 | tf_op jit(solution)/shard_map/load/pallas_call | solution.py:146
  35.5 1.5 %collective-permute-done.10.first_ref = bf16[64,2176]{1,0:T(8,128)(2,1)} collective-permute-done((bf16[64,2176]{1,0:T(8,128)(2,1)S(1)}, bf16[64,2176]{1,0:T(8,128)(2,1)}, u32[]{:S(2)}, u32[]{:S(2)}) %collective-permute-start.10) | collective-permute-done | bytes 278560 | tf_op jit(solution)/shard_map/ppermute | solution.py:355
  37.0 4.7 %collective-permute-done.11.second_ref = bf16[64,2176]{1,0:T(8,128)(2,1)} collective-permute-done((bf16[64,2176]{1,0:T(8,128)(2,1)S(1)}, bf16[64,2176]{1,0:T(8,128)(2,1)}, u32[]{:S(2)}, u32[]{:S(2)}) %collective-permute-start.11) | collective-permute-done | bytes 278560 | tf_op jit(solution)/shard_map/ppermute | solution.py:355
  41.8 2.9 %routed_rows.3 = (bf16[64,2048]{1,0:T(8,128)(2,1)S(1)}, bf16[64,2048]{1,0:T(8,128)(2,1)S(1)}) custom-call(s32[2]{0:T(128)S(1)} %pad_add_fusion.place_ref, bf16[64,2176]{1,0:T(8,128)(2,1)} %collective-permute-done.10.first_ref, bf16[64,2176]{1,0:T(8,128)(2,1)} %collective-permute-done.11.second_ref, bf16[1,2048]{1,0:T(2,128)(2,1)S(1)} %broadcast_in_dim.20.branch_ref, ...), custom_call_target="tpu_custom_call" | custom-call | flops 805306368 | bytes 8388608 | tf_op jit(solution)/shard_map/routed_rows/pallas_call | solution.py:301
  44.6 0.8 %collective-permute-start.12 = (bf16[64,2048]{1,0:T(8,128)(2,1)S(1)}, bf16[64,2048]{1,0:T(8,128)(2,1)S(1)}, u32[]{:S(2)}, u32[]{:S(2)}) collective-permute-start(bf16[64,2048]{1,0:T(8,128)(2,1)S(1)} %get-tuple-element.28), channel_id=1, source_target_pairs={{2,0},{3,1},{0,2},{1,3},{6,4},{7,5},{4,6},{5,7},{10,8},{11,9},{8,1... | collective-permute-start | bytes 786440 | tf_op jit(solution)/shard_map/ppermute | solution.py:355
  45.4 1.4 %collective-permute-start.13 = (bf16[64,2048]{1,0:T(8,128)(2,1)S(1)}, bf16[64,2048]{1,0:T(8,128)(2,1)S(1)}, u32[]{:S(2)}, u32[]{:S(2)}) collective-permute-start(bf16[64,2048]{1,0:T(8,128)(2,1)S(1)} %get-tuple-element.29), channel_id=1, source_target_pairs={{4,0},{5,1},{6,2},{7,3},{0,4},{1,5},{2,6},{3,7},{12,8},{13,9},{14,... | collective-permute-start | bytes 786440 | tf_op jit(solution)/shard_map/ppermute | solution.py:355
  46.8 2.8 %routed_rows.2 = (bf16[64,2048]{1,0:T(8,128)(2,1)S(1)}, bf16[64,2048]{1,0:T(8,128)(2,1)S(1)}) custom-call(s32[2]{0:T(128)S(1)} %pad_add_fusion.place_ref, bf16[64,2176]{1,0:T(8,128)(2,1)} %collective-permute-done.5.first_ref, bf16[64,2176]{1,0:T(8,128)(2,1)S(1)} %join.1.second_ref, bf16[1,2048]{1,0:T(2,128)(2,1)S(1)} %broadcast_in_dim.20.branch_ref, ...), custom_call_target="tpu_custom_call" | custom-call | flops 805306368 | bytes 8388608 | tf_op jit(solution)/shard_map/routed_rows/pallas_call | solution.py:301
  49.6 1.7 %collective-permute-start.14 = (bf16[64,2048]{1,0:T(8,128)(2,1)S(1)}, bf16[64,2048]{1,0:T(8,128)(2,1)S(1)}, u32[]{:S(2)}, u32[]{:S(2)}) collective-permute-start(bf16[64,2048]{1,0:T(8,128)(2,1)S(1)} %get-tuple-element.30), channel_id=1, source_target_pairs={{6,0},{7,1},{4,2},{5,3},{2,4},{3,5},{0,6},{1,7},{14,8},{15,9},{12,... | collective-permute-start | bytes 786440 | tf_op jit(solution)/shard_map/ppermute | solution.py:355
  51.3 1.3 %collective-permute-done.18.far_ref = bf16[16,2176]{1,0:T(8,128)(2,1)S(1)} collective-permute-done((bf16[16,2176]{1,0:T(8,128)(2,1)S(1)}, bf16[16,2176]{1,0:T(8,128)(2,1)S(1)}, u32[]{:S(2)}, u32[]{:S(2)}) %collective-permute-start.18) | collective-permute-done | bytes 69664 | tf_op jit(solution)/shard_map/ppermute | solution.py:352
  52.6 1.3 %shared_mlp.1 = (bf16[16,2048]{1,0:T(8,128)(2,1)S(1)}, bf16[16,2048]{1,0:T(8,128)(2,1)S(1)}) custom-call(bf16[16,2176]{1,0:T(8,128)(2,1)S(1)} %mix.1.refs_0_.own_ref.packet_ref, bf16[16,2176]{1,0:T(8,128)(2,1)S(1)} %collective-permute-done.18.far_ref, bf16[2048,256]{1,0:T(8,128)(2,1)S(1)} %copy-done.4, bf16[2048,256]{1,0:T(8,128)(2,1)S(1)} %copy-done.5, ...), custom_call_target="tpu_custom_call" | custom-call | flops 100663296 | bytes 3145728 | tf_op jit(solution)/shard_map/shared_mlp/pallas_call | solution.py:448
  54.2 2.8 %collective-permute-done.14.refs_3_ = bf16[64,2048]{1,0:T(8,128)(2,1)S(1)} collective-permute-done((bf16[64,2048]{1,0:T(8,128)(2,1)S(1)}, bf16[64,2048]{1,0:T(8,128)(2,1)S(1)}, u32[]{:S(2)}, u32[]{:S(2)}) %collective-permute-start.14) | collective-permute-done | bytes 262176 | tf_op jit(solution)/shard_map/ppermute | solution.py:355
  57.0 1.0 %collective-permute-start.15 = (bf16[16,2048]{1,0:T(8,128)(2,1)S(1)}, bf16[16,2048]{1,0:T(8,128)(2,1)S(1)}, u32[]{:S(2)}, u32[]{:S(2)}) collective-permute-start(bf16[16,2048]{1,0:T(8,128)(2,1)S(1)} %get-tuple-element.32), channel_id=1, source_target_pairs={{8,0},{9,1},{10,2},{11,3},{12,4},{13,5},{14,6},{15,7},{0,8},{1,9},... | collective-permute-start | bytes 196616 | tf_op jit(solution)/shard_map/ppermute | solution.py:355
  58.1 3.1 %collective-permute-start.16 = (bf16[16,2048]{1,0:T(8,128)(2,1)S(1)}, bf16[16,2048]{1,0:T(8,128)(2,1)S(1)}, u32[]{:S(2)}, u32[]{:S(2)}) collective-permute-start(bf16[16,2048]{1,0:T(8,128)(2,1)S(1)} %get-tuple-element.33), channel_id=1, source_target_pairs={{16,0},{17,1},{18,2},{19,3},{20,4},{21,5},{22,6},{23,7},{24,8},{25... | collective-permute-start | bytes 196616 | tf_op jit(solution)/shard_map/ppermute | solution.py:355
  61.6 1.2 %collective-permute-done.1.far_norm_ref = f32[2,1024]{1,0:T(2,128)S(1)} collective-permute-done((f32[2,1024]{1,0:T(2,128)S(1)}, f32[2,1024]{1,0:T(2,128)S(1)}, u32[]{:S(2)}, u32[]{:S(2)}) %collective-permute-start.1) | collective-permute-done | bytes 8224 | tf_op jit(solution)/shard_map/ppermute | solution.py:352
  62.8 2.0 %collective-permute-done.16.refs_2_ = bf16[16,2048]{1,0:T(8,128)(2,1)S(1)} collective-permute-done((bf16[16,2048]{1,0:T(8,128)(2,1)S(1)}, bf16[16,2048]{1,0:T(8,128)(2,1)S(1)}, u32[]{:S(2)}, u32[]{:S(2)}) %collective-permute-start.16) | collective-permute-done | bytes 65568 | tf_op jit(solution)/shard_map/ppermute | solution.py:355
  64.8 2.5 %collective-permute-done.17.refs_3_ = bf16[16,2048]{1,0:T(8,128)(2,1)S(1)} collective-permute-done((bf16[16,2048]{1,0:T(8,128)(2,1)S(1)}, bf16[16,2048]{1,0:T(8,128)(2,1)S(1)}, u32[]{:S(2)}, u32[]{:S(2)}) %collective-permute-start.17) | collective-permute-done | bytes 65568 | tf_op jit(solution)/shard_map/ppermute | solution.py:355
  67.5 1.2 %collective-permute-done.20.far_ref = bf16[16,1024]{1,0:T(8,128)(2,1)S(1)} collective-permute-done((bf16[16,1024]{1,0:T(8,128)(2,1)S(1)}, bf16[16,1024]{1,0:T(8,128)(2,1)S(1)}, u32[]{:S(2)}, u32[]{:S(2)}) %collective-permute-start.20) | collective-permute-done | bytes 32800 | tf_op jit(solution)/shard_map/ppermute | solution.py:352
  68.7 0.6 place.1
  (65 shorter events, 3.2 us)
Async XLA Ops:
  0.6 9.1 %copy-start.9 = (bf16[32,2048]{1,0:T(8,128)(2,1)S(1)}, bf16[32,2048]{1,0:T(8,128)(2,1)}, u32[]{:S(2)}) copy-start(bf16[32,2048]{1,0:T(8,128)(2,1)} %input_ref.1) | copy-start | bytes 393220
  0.7 9.1 %copy-start.8 = (bf16[512,512]{1,0:T(8,128)(2,1)S(1)}, bf16[512,512]{1,0:T(8,128)(2,1)}, u32[]{:S(2)}) copy-start(bf16[512,512]{1,0:T(8,128)(2,1)} %glu_ref.1) | copy-start | bytes 1572868
  0.7 9.1 %copy-start.12 = (f32[2048]{0:T(1024)S(1)}, f32[2048]{0:T(1024)}, u32[]{:S(2)}) copy-start(f32[2048]{0:T(1024)} %param.37) | copy-start | bytes 24580
  0.7 9.1 %copy-start.13 = (f32[2048]{0:T(1024)S(1)}, f32[2048]{0:T(1024)}, u32[]{:S(2)}) copy-start(f32[2048]{0:T(1024)} %param.38) | copy-start | bytes 24580
  0.7 31.5 %collective-permute-start.6 = (bf16[1,2048,256]{2,1,0:T(8,128)(2,1)}, bf16[1,2048,256]{2,1,0:T(8,128)(2,1)}, u32[]{:S(2)}, u32[]{:S(2)}) collective-permute-start(bf16[1,2048,256]{2,1,0:T(8,128)(2,1)} %refs_0_.3), channel_id=1, source_target_pairs={{0,1},{1,0},{2,3},{3,2},{4,5},{5,4},{6,7},{7,6},{8,9},{9,8},{10,11... | collective-permute-start | bytes 3145736 | tf_op jit(solution)/shard_map/ppermute | solution.py:352
  1.3 31.5 %collective-permute-start.7 = (bf16[1,2048,256]{2,1,0:T(8,128)(2,1)}, bf16[1,2048,256]{2,1,0:T(8,128)(2,1)}, u32[]{:S(2)}, u32[]{:S(2)}) collective-permute-start(bf16[1,2048,256]{2,1,0:T(8,128)(2,1)} %refs_1_.5), channel_id=1, source_target_pairs={{0,1},{1,0},{2,3},{3,2},{4,5},{5,4},{6,7},{7,6},{8,9},{9,8},{10,11... | collective-permute-start | bytes 3145736 | tf_op jit(solution)/shard_map/ppermute | solution.py:352
  1.3 31.4 %collective-permute-start.8 = (bf16[1,256,2048]{2,1,0:T(8,128)(2,1)}, bf16[1,256,2048]{2,1,0:T(8,128)(2,1)}, u32[]{:S(2)}, u32[]{:S(2)}) collective-permute-start(bf16[1,256,2048]{2,1,0:T(8,128)(2,1)} %refs_4_.5), channel_id=1, source_target_pairs={{0,1},{1,0},{2,3},{3,2},{4,5},{5,4},{6,7},{7,6},{8,9},{9,8},{10,11... | collective-permute-start | bytes 3145736 | tf_op jit(solution)/shard_map/ppermute | solution.py:352
  8.3 24.3 %copy-start.17 = (bf16[2048]{0:T(1024)(128)(2,1)S(1)}, bf16[2048]{0:T(1024)(128)(2,1)}, u32[]{:S(2)}) copy-start(bf16[2048]{0:T(1024)(128)(2,1)} %param.49) | copy-start | bytes 12292
  8.3 1.4 %collective-permute-start = (bf16[16,256]{1,0:T(8,128)(2,1)}, bf16[16,256]{1,0:T(8,128)(2,1)S(1)}, u32[]{:S(2)}, u32[]{:S(2)}) collective-permute-start(bf16[16,256]{1,0:T(8,128)(2,1)} %get-tuple-element.22), channel_id=1, source_target_pairs={{0,1},{1,0},{2,3},{3,2},{4,5},{5,4},{6,7},{7,6},{8,9},{9,8},{10,11... | collective-permute-start | bytes 24584 | tf_op jit(solution)/shard_map/ppermute | solution.py:352
  12.9 28.9 %copy-start = (bf16[1,2048,256]{2,1,0:T(8,128)(2,1)S(1)}, bf16[1,2048,256]{2,1,0:T(8,128)(2,1)}, u32[]{:S(2)}) copy-start(bf16[1,2048,256]{2,1,0:T(8,128)(2,1)} %refs_0_.3) | copy-start | bytes 3145732
  12.9 28.9 %copy-start.1 = (bf16[1,2048,256]{2,1,0:T(8,128)(2,1)S(1)}, bf16[1,2048,256]{2,1,0:T(8,128)(2,1)}, u32[]{:S(2)}) copy-start(bf16[1,2048,256]{2,1,0:T(8,128)(2,1)} %refs_1_.5) | copy-start | bytes 3145732
  12.9 28.9 %copy-start.2 = (bf16[1,256,2048]{2,1,0:T(8,128)(2,1)S(1)}, bf16[1,256,2048]{2,1,0:T(8,128)(2,1)}, u32[]{:S(2)}) copy-start(bf16[1,256,2048]{2,1,0:T(8,128)(2,1)} %refs_4_.5) | copy-start | bytes 3145732
  12.9 5.5 %collective-permute-start.2 = (bf16[16,2176]{1,0:T(8,128)(2,1)S(1)}, bf16[16,2176]{1,0:T(8,128)(2,1)S(1)}, u32[]{:S(2)}, u32[]{:S(2)}) collective-permute-start(bf16[16,2176]{1,0:T(8,128)(2,1)S(1)} %mix.1.refs_0_.own_ref.packet_ref), channel_id=1, source_target_pairs={{0,8},{1,9},{2,10},{3,11},{4,12},{5,13},{6,14},{7,15},{8,0},{9,1},... | collective-permute-start | bytes 208904 | tf_op jit(solution)/shard_map/ppermute | solution.py:355
  15.7 6.6 %collective-permute-start.3 = (bf16[16,2176]{1,0:T(8,128)(2,1)S(1)}, bf16[16,2176]{1,0:T(8,128)(2,1)S(1)}, u32[]{:S(2)}, u32[]{:S(2)}) collective-permute-start(bf16[16,2176]{1,0:T(8,128)(2,1)S(1)} %mix.1.refs_0_.own_ref.packet_ref), channel_id=1, source_target_pairs={{0,16},{1,17},{2,18},{3,19},{4,20},{5,21},{6,22},{7,23},{8,24},{9,... | collective-permute-start | bytes 208904 | tf_op jit(solution)/shard_map/ppermute | solution.py:355
  18.4 11.6 %collective-permute-start.9 = (bf16[64,1024]{1,0:T(8,128)(2,1)}, bf16[64,1024]{1,0:T(8,128)(2,1)S(1)}, u32[]{:S(2)}, u32[]{:S(2)}) collective-permute-start(bf16[64,1024]{1,0:T(8,128)(2,1)} %refs_7_.5), channel_id=1, source_target_pairs={{0,1},{1,0},{2,3},{3,2},{4,5},{5,4},{6,7},{7,6},{8,9},{9,8},{10,11... | collective-permute-start | bytes 393224 | tf_op jit(solution)/shard_map/ppermute | solution.py:352
  22.3 6.1 %collective-permute-start.4 = (bf16[16,2176]{1,0:T(8,128)(2,1)S(1)}, bf16[16,2176]{1,0:T(8,128)(2,1)S(1)}, u32[]{:S(2)}, u32[]{:S(2)}) collective-permute-start(bf16[16,2176]{1,0:T(8,128)(2,1)S(1)} %mix.1.refs_0_.own_ref.packet_ref), channel_id=1, source_target_pairs={{0,24},{1,25},{2,26},{3,27},{4,28},{5,29},{6,30},{7,31},{8,16},{9,... | collective-permute-start | bytes 208904 | tf_op jit(solution)/shard_map/ppermute | solution.py:355
  28.4 8.6 %collective-permute-start.10 = (bf16[64,2176]{1,0:T(8,128)(2,1)S(1)}, bf16[64,2176]{1,0:T(8,128)(2,1)}, u32[]{:S(2)}, u32[]{:S(2)}) collective-permute-start(bf16[64,2176]{1,0:T(8,128)(2,1)S(1)} %join.1.second_ref), channel_id=1, source_target_pairs={{0,2},{1,3},{2,0},{3,1},{4,6},{5,7},{6,4},{7,5},{8,10},{9,11},{10,... | collective-permute-start | bytes 835592 | tf_op jit(solution)/shard_map/ppermute | solution.py:355
  30.6 11.1 %collective-permute-start.11 = (bf16[64,2176]{1,0:T(8,128)(2,1)S(1)}, bf16[64,2176]{1,0:T(8,128)(2,1)}, u32[]{:S(2)}, u32[]{:S(2)}) collective-permute-start(bf16[64,2176]{1,0:T(8,128)(2,1)S(1)} %join.1.second_ref), channel_id=1, source_target_pairs={{0,4},{1,5},{2,6},{3,7},{4,0},{5,1},{6,2},{7,3},{8,12},{9,13},{10,... | collective-permute-start | bytes 835592 | tf_op jit(solution)/shard_map/ppermute | solution.py:355
  32.2 14.6 %collective-permute-start.5 = (bf16[64,2176]{1,0:T(8,128)(2,1)S(1)}, bf16[64,2176]{1,0:T(8,128)(2,1)}, u32[]{:S(2)}, u32[]{:S(2)}) collective-permute-start(bf16[64,2176]{1,0:T(8,128)(2,1)S(1)} %join.1.second_ref), channel_id=1, source_target_pairs={{0,6},{1,7},{2,4},{3,5},{4,2},{5,3},{6,0},{7,1},{8,14},{9,15},{10,... | collective-permute-start | bytes 835592 | tf_op jit(solution)/shard_map/ppermute | solution.py:355
  32.6 9.1 %copy-start.7 = (bf16[64,2048]{1,0:T(8,128)(2,1)S(1)}, bf16[64,2048]{1,0:T(8,128)(2,1)}, u32[]{:S(2)}) copy-start(bf16[64,2048]{1,0:T(8,128)(2,1)} %refs_6_.3) | copy-start | bytes 786436
  44.6 9.5 %collective-permute-start.12 = (bf16[64,2048]{1,0:T(8,128)(2,1)S(1)}, bf16[64,2048]{1,0:T(8,128)(2,1)S(1)}, u32[]{:S(2)}, u32[]{:S(2)}) collective-permute-start(bf16[64,2048]{1,0:T(8,128)(2,1)S(1)} %get-tuple-element.28), channel_id=1, source_target_pairs={{2,0},{3,1},{0,2},{1,3},{6,4},{7,5},{4,6},{5,7},{10,8},{11,9},{8,1... | collective-permute-start | bytes 786440 | tf_op jit(solution)/shard_map/ppermute | solution.py:355
  45.4 8.8 %collective-permute-start.13 = (bf16[64,2048]{1,0:T(8,128)(2,1)S(1)}, bf16[64,2048]{1,0:T(8,128)(2,1)S(1)}, u32[]{:S(2)}, u32[]{:S(2)}) collective-permute-start(bf16[64,2048]{1,0:T(8,128)(2,1)S(1)} %get-tuple-element.29), channel_id=1, source_target_pairs={{4,0},{5,1},{6,2},{7,3},{0,4},{1,5},{2,6},{3,7},{12,8},{13,9},{14,... | collective-permute-start | bytes 786440 | tf_op jit(solution)/shard_map/ppermute | solution.py:355
  49.6 12.0 %copy-start.18 = (f32[1024]{0:T(1024)S(1)}, f32[1024]{0:T(1024)}, u32[]{:S(2)}) copy-start(f32[1024]{0:T(1024)} %param.51) | copy-start | bytes 12292
  49.6 11.9 %copy-start.19 = (f32[1024]{0:T(1024)S(1)}, f32[1024]{0:T(1024)}, u32[]{:S(2)}) copy-start(f32[1024]{0:T(1024)} %param.50) | copy-start | bytes 12292
  49.6 7.3 %collective-permute-start.14 = (bf16[64,2048]{1,0:T(8,128)(2,1)S(1)}, bf16[64,2048]{1,0:T(8,128)(2,1)S(1)}, u32[]{:S(2)}, u32[]{:S(2)}) collective-permute-start(bf16[64,2048]{1,0:T(8,128)(2,1)S(1)} %get-tuple-element.30), channel_id=1, source_target_pairs={{6,0},{7,1},{4,2},{5,3},{2,4},{3,5},{0,6},{1,7},{14,8},{15,9},{12,... | collective-permute-start | bytes 786440 | tf_op jit(solution)/shard_map/ppermute | solution.py:355
  51.3 1.3 %collective-permute-start.18 = (bf16[16,2176]{1,0:T(8,128)(2,1)S(1)}, bf16[16,2176]{1,0:T(8,128)(2,1)S(1)}, u32[]{:S(2)}, u32[]{:S(2)}) collective-permute-start(bf16[16,2176]{1,0:T(8,128)(2,1)S(1)} %mix.1.refs_0_.own_ref.packet_ref), channel_id=1, source_target_pairs={{0,1},{1,0},{2,3},{3,2},{4,5},{5,4},{6,7},{7,6},{8,9},{9,8},{10,11... | collective-permute-start | bytes 208904 | tf_op jit(solution)/shard_map/ppermute | solution.py:352
  53.9 8.8 %collective-permute-start.19 = (bf16[16,2048]{1,0:T(8,128)(2,1)S(1)}, bf16[16,2048]{1,0:T(8,128)(2,1)S(1)}, u32[]{:S(2)}, u32[]{:S(2)}) collective-permute-start(bf16[16,2048]{1,0:T(8,128)(2,1)S(1)} %get-tuple-element.36), channel_id=1, source_target_pairs={{0,1},{1,0},{2,3},{3,2},{4,5},{5,4},{6,7},{7,6},{8,9},{9,8},{10,11... | collective-permute-start | bytes 196616 | tf_op jit(solution)/shard_map/ppermute | solution.py:352
  57.0 5.7 %collective-permute-start.15 = (bf16[16,2048]{1,0:T(8,128)(2,1)S(1)}, bf16[16,2048]{1,0:T(8,128)(2,1)S(1)}, u32[]{:S(2)}, u32[]{:S(2)}) collective-permute-start(bf16[16,2048]{1,0:T(8,128)(2,1)S(1)} %get-tuple-element.32), channel_id=1, source_target_pairs={{8,0},{9,1},{10,2},{11,3},{12,4},{13,5},{14,6},{15,7},{0,8},{1,9},... | collective-permute-start | bytes 196616 | tf_op jit(solution)/shard_map/ppermute | solution.py:355
  58.1 6.7 %collective-permute-start.16 = (bf16[16,2048]{1,0:T(8,128)(2,1)S(1)}, bf16[16,2048]{1,0:T(8,128)(2,1)S(1)}, u32[]{:S(2)}, u32[]{:S(2)}) collective-permute-start(bf16[16,2048]{1,0:T(8,128)(2,1)S(1)} %get-tuple-element.33), channel_id=1, source_target_pairs={{16,0},{17,1},{18,2},{19,3},{20,4},{21,5},{22,6},{23,7},{24,8},{25... | collective-permute-start | bytes 196616 | tf_op jit(solution)/shard_map/ppermute | solution.py:355
  61.2 6.1 %collective-permute-start.17 = (bf16[16,2048]{1,0:T(8,128)(2,1)S(1)}, bf16[16,2048]{1,0:T(8,128)(2,1)S(1)}, u32[]{:S(2)}, u32[]{:S(2)}) collective-permute-start(bf16[16,2048]{1,0:T(8,128)(2,1)S(1)} %get-tuple-element.34), channel_id=1, source_target_pairs={{24,0},{25,1},{26,2},{27,3},{28,4},{29,5},{30,6},{31,7},{16,8},{17... | collective-permute-start | bytes 196616 | tf_op jit(solution)/shard_map/ppermute | solution.py:355
  61.5 1.2 %collective-permute-start.1 = (f32[2,1024]{1,0:T(2,128)S(1)}, f32[2,1024]{1,0:T(2,128)S(1)}, u32[]{:S(2)}, u32[]{:S(2)}) collective-permute-start(f32[2,1024]{1,0:T(2,128)S(1)} %pad_maximum_fusion.own_norm_ref), channel_id=1, source_target_pairs={{0,1},{1,0},{2,3},{3,2},{4,5},{5,4},{6,7},{7,6},{8,9},{9,8},{10,11... | collective-permute-start | bytes 24584 | tf_op jit(solution)/shard_map/ppermute | solution.py:352
  67.5 1.3 %collective-permute-start.20 = (bf16[16,1024]{1,0:T(8,128)(2,1)S(1)}, bf16[16,1024]{1,0:T(8,128)(2,1)S(1)}, u32[]{:S(2)}, u32[]{:S(2)}) collective-permute-start(bf16[16,1024]{1,0:T(8,128)(2,1)S(1)} %get-tuple-element.38), channel_id=1, source_target_pairs={{0,1},{1,0},{2,3},{3,2},{4,5},{5,4},{6,7},{7,6},{8,9},{9,8},{10,11... | collective-permute-start | bytes 98312 | tf_op jit(solution)/shard_map/ppermute | solution.py:352
  (9 other events, 41.2 us)

commit v3 on v2

--- a/solution.py
+++ b/solution.py
@@ -35,9 +35,13 @@
 
 
 def plane_moves(step, count_ep, count_tp):
+    inner = split_of(count_ep)[1]
     moves = []
     for rank in range(count_ep):
-        moves += [(rank * count_tp + t, (rank ^ step) * count_tp + t) for t in range(count_tp)]
+        for t in range(count_tp):
+            crossed = inner == 4 and step < 3 and t % 2 == 1
+            peer = rank ^ (3 - step if crossed else step)
+            moves.append((rank * count_tp + t, peer * count_tp + t))
     return moves
 
 

time: 69.7 us -> 69.9 us (level)
  starting transfers between devices: 21.4 us -> 22.1 us
  transfers between devices with their start and end apart: 21 -> 21, of which waited for: 12 -> 12; matrix products, arithmetic and copies ran while one was open for 0% -> 0% of each run, Pallas kernels for 24% -> 23%
where the time goes in v3:
time: 69.9 us; the launch traced here: 69.6 us
  waiting for transfers between devices  25.3 us (36%)
  starting transfers between devices  22.1 us (32%)
  Pallas kernels  17.1 us (24%)
  local copies, waits for them, and re-layouts  4.11 us (6%)
  between operations  0.92 us (1%)
    ppermute x12, waiting for transfers between devices, moved(): return lax.ppermute(value, both_axes, moves)  20.6 us
    ppermute x12, starting transfers between devices, moved(): return lax.ppermute(value, both_axes, moves)  20.5 us
    pallas_call x1, Pallas kernels, body(): pl.pallas_call(mixer_kernel, out_shape=[half_channels, half_channels, jax...  6.54 us
    pallas_call x2, Pallas kernels, routed_rows(): pl.pallas_call(functools.partial(routed_kernel, width, experts, weights[0...  5.65 us
    ppermute x9, waiting for transfers between devices, swapped(): return lax.ppermute(value, 'tp', [(t, 1 - t) for t in range(count_tp)])  4.74 us
    unnamed x42, local copies, waits for them, and re-layouts  4.1 us
    pallas_call x1, Pallas kernels, loaded(): pl.pallas_call(functools.partial(load_kernel, len(values)), out_shape=[ja...  1.89 us
    ppermute x9, starting transfers between devices, swapped(): return lax.ppermute(value, 'tp', [(t, 1 - t) for t in range(count_tp)])  1.58 us
  transfers between devices with their start and end apart: 21, of which 12 were waited for; matrix products, arithmetic and copies ran while one was open for 0% of the time, Pallas kernels for 23%

profile of v3, /device:TPU:0, one launch (start us, length us, event | category | flops | bytes accessed | tf_op | source)
XLA Modules:
  0.0 69.6 jit_solution(16058341394925815862)
XLA Ops:
  0.7 0.6 collective-permute-start.6
  1.8 6.5 %mixer.1 = (bf16[16,256]{1,0:T(8,128)(2,1)}, bf16[16,256]{1,0:T(8,128)(2,1)}, f32[1024,64]{1,0:T(8,128)}) custom-call(s32[1]{0:T(128)} %bitcast.core_ref, f32[1,16]{1,0:T(1,128)} %bitcast.16, f32[16,64]{1,0:T(8,128)} %refs_1_.3, f32[16,64]{1,0:T(8,128)} %refs_2_.1, bf16[32,2048]{1,0:T(8,128)(2,1)} %input_ref.1, bf16[2048,256]{1,0:T(8,128)(2,1)} %refs_4_.3, ...), custom_call_target="tpu_custom_call" | custom-call | flops 67108864 | bytes 5242880 | tf_op jit(solution)/shard_map/mixer/pallas_call | solution.py:381
  8.7 1.1 %collective-permute-done.far_ref = bf16[16,256]{1,0:T(8,128)(2,1)S(1)} collective-permute-done((bf16[16,256]{1,0:T(8,128)(2,1)}, bf16[16,256]{1,0:T(8,128)(2,1)S(1)}, u32[]{:S(2)}, u32[]{:S(2)}) %collective-permute-start) | collective-permute-done | bytes 8224 | tf_op jit(solution)/shard_map/ppermute | solution.py:356
  9.8 1.6 %copy-done.3 = bf16[512,2048]{1,0:T(8,128)(2,1)S(1)} copy-done((bf16[512,2048]{1,0:T(8,128)(2,1)S(1)}, bf16[512,2048]{1,0:T(8,128)(2,1)}, u32[]{:S(2)}) %copy-start.3) | copy-done | bytes 2097176
  11.4 0.7 copy-done.14
  12.1 0.8 %mix.1.refs_0_.own_ref.packet_ref = bf16[16,2176]{1,0:T(8,128)(2,1)S(1)} custom-call(s32[1]{0:T(128)} %bitcast.core_ref, bf16[16,256]{1,0:T(8,128)(2,1)S(1)} %copy-done.14, bf16[16,256]{1,0:T(8,128)(2,1)S(1)} %collective-permute-done.far_ref, bf16[512,512]{1,0:T(8,128)(2,1)S(1)} %copy-done.8, bf16[512,2048]{1,0:T(8,128)(2,1)S(1)} %copy-done.3, ...), custom_call_target="tpu_custom_call" | custom-call | flops 83886080 | bytes 3145728 | tf_op jit(solution)/shard_map/mix/pallas_call | solution.py:401
  12.9 2.8 %collective-permute-start.2 = (bf16[16,2176]{1,0:T(8,128)(2,1)S(1)}, bf16[16,2176]{1,0:T(8,128)(2,1)S(1)}, u32[]{:S(2)}, u32[]{:S(2)}) collective-permute-start(bf16[16,2176]{1,0:T(8,128)(2,1)S(1)} %mix.1.refs_0_.own_ref.packet_ref), channel_id=1, source_target_pairs={{0,8},{1,9},{2,10},{3,11},{4,12},{5,13},{6,14},{7,15},{8,0},{9,1},... | collective-permute-start | bytes 208904 | tf_op jit(solution)/shard_map/ppermute | solution.py:359
  15.7 2.6 %collective-permute-start.3 = (bf16[16,2176]{1,0:T(8,128)(2,1)S(1)}, bf16[16,2176]{1,0:T(8,128)(2,1)S(1)}, u32[]{:S(2)}, u32[]{:S(2)}) collective-permute-start(bf16[16,2176]{1,0:T(8,128)(2,1)S(1)} %mix.1.refs_0_.own_ref.packet_ref), channel_id=1, source_target_pairs={{0,16},{1,17},{2,18},{3,19},{4,20},{5,21},{6,22},{7,23},{8,24},{9,... | collective-permute-start | bytes 208904 | tf_op jit(solution)/shard_map/ppermute | solution.py:359
  18.4 3.9 %collective-permute-done.3.refs_2_ = bf16[16,2176]{1,0:T(8,128)(2,1)S(1)} collective-permute-done((bf16[16,2176]{1,0:T(8,128)(2,1)S(1)}, bf16[16,2176]{1,0:T(8,128)(2,1)S(1)}, u32[]{:S(2)}, u32[]{:S(2)}) %collective-permute-start.3) | collective-permute-done | bytes 69664 | tf_op jit(solution)/shard_map/ppermute | solution.py:359
  22.3 2.6 %collective-permute-start.4 = (bf16[16,2176]{1,0:T(8,128)(2,1)S(1)}, bf16[16,2176]{1,0:T(8,128)(2,1)S(1)}, u32[]{:S(2)}, u32[]{:S(2)}) collective-permute-start(bf16[16,2176]{1,0:T(8,128)(2,1)S(1)} %mix.1.refs_0_.own_ref.packet_ref), channel_id=1, source_target_pairs={{0,24},{1,25},{2,26},{3,27},{4,28},{5,29},{6,30},{7,31},{8,16},{9,... | collective-permute-start | bytes 208904 | tf_op jit(solution)/shard_map/ppermute | solution.py:359
  24.9 3.5 %collective-permute-done.4.refs_3_ = bf16[16,2176]{1,0:T(8,128)(2,1)S(1)} collective-permute-done((bf16[16,2176]{1,0:T(8,128)(2,1)S(1)}, bf16[16,2176]{1,0:T(8,128)(2,1)S(1)}, u32[]{:S(2)}, u32[]{:S(2)}) %collective-permute-start.4) | collective-permute-done | bytes 69664 | tf_op jit(solution)/shard_map/ppermute | solution.py:359
  28.4 1.6 %collective-permute-start.10 = (bf16[64,2176]{1,0:T(8,128)(2,1)S(1)}, bf16[64,2176]{1,0:T(8,128)(2,1)}, u32[]{:S(2)}, u32[]{:S(2)}) collective-permute-start(bf16[64,2176]{1,0:T(8,128)(2,1)S(1)} %join.1.second_ref), channel_id=1, source_target_pairs={{0,2},{1,5},{2,0},{3,7},{4,6},{5,1},{6,4},{7,3},{8,10},{9,13},{10,... | collective-permute-start | bytes 835592 | tf_op jit(solution)/shard_map/ppermute | solution.py:359
  30.0 0.7 copy-done.10
  30.6 1.5 %collective-permute-start.11 = (bf16[64,2176]{1,0:T(8,128)(2,1)S(1)}, bf16[64,2176]{1,0:T(8,128)(2,1)}, u32[]{:S(2)}, u32[]{:S(2)}) collective-permute-start(bf16[64,2176]{1,0:T(8,128)(2,1)S(1)} %join.1.second_ref), channel_id=1, source_target_pairs={{0,4},{1,3},{2,6},{3,1},{4,0},{5,7},{6,2},{7,5},{8,12},{9,11},{10,... | collective-permute-start | bytes 835592 | tf_op jit(solution)/shard_map/ppermute | solution.py:359
  32.7 0.9 %copy-done.11 = bf16[64,1024]{1,0:T(8,128)(2,1)S(1)} copy-done((bf16[64,1024]{1,0:T(8,128)(2,1)S(1)}, bf16[64,1024]{1,0:T(8,128)(2,1)}, u32[]{:S(2)}) %copy-start.11) | copy-done | bytes 131096
  33.6 1.9 %load.1 = (bf16[1,2048,256]{2,1,0:T(8,128)(2,1)S(1)}, bf16[1,2048,256]{2,1,0:T(8,128)(2,1)S(1)}, bf16[1,256,2048]{2,1,0:T(8,128)(2,1)S(1)}, bf16[64,1024]{1,0:T(8,128)(2,1)S(1)}) custom-call(bf16[1,2048,256]{2,1,0:T(8,128)(2,1)} %collective-permute-done.6.refs_0_, bf16[1,2048,256]{2,1,0:T(8,128)(2,1)} %collective-permute-done.7.refs_1_, ...), custom_call_target="tpu_custom_call" | custom-call | flops 4194304 | bytes 8388608 | tf_op jit(solution)/shard_map/load/pallas_call | solution.py:150
  35.5 2.6 %collective-permute-done.10.first_ref = bf16[64,2176]{1,0:T(8,128)(2,1)} collective-permute-done((bf16[64,2176]{1,0:T(8,128)(2,1)S(1)}, bf16[64,2176]{1,0:T(8,128)(2,1)}, u32[]{:S(2)}, u32[]{:S(2)}) %collective-permute-start.10) | collective-permute-done | bytes 278560 | tf_op jit(solution)/shard_map/ppermute | solution.py:359
  38.1 4.4 %collective-permute-done.11.second_ref = bf16[64,2176]{1,0:T(8,128)(2,1)} collective-permute-done((bf16[64,2176]{1,0:T(8,128)(2,1)S(1)}, bf16[64,2176]{1,0:T(8,128)(2,1)}, u32[]{:S(2)}, u32[]{:S(2)}) %collective-permute-start.11) | collective-permute-done | bytes 278560 | tf_op jit(solution)/shard_map/ppermute | solution.py:359
  42.6 2.9 %routed_rows.3 = (bf16[64,2048]{1,0:T(8,128)(2,1)S(1)}, bf16[64,2048]{1,0:T(8,128)(2,1)S(1)}) custom-call(s32[2]{0:T(128)S(1)} %pad_add_fusion.place_ref, bf16[64,2176]{1,0:T(8,128)(2,1)} %collective-permute-done.10.first_ref, bf16[64,2176]{1,0:T(8,128)(2,1)} %collective-permute-done.11.second_ref, bf16[1,2048]{1,0:T(2,128)(2,1)S(1)} %broadcast_in_dim.20.branch_ref, ...), custom_call_target="tpu_custom_call" | custom-call | flops 805306368 | bytes 8388608 | tf_op jit(solution)/shard_map/routed_rows/pallas_call | solution.py:305
  45.5 2.9 %collective-permute-start.13 = (bf16[64,2048]{1,0:T(8,128)(2,1)S(1)}, bf16[64,2048]{1,0:T(8,128)(2,1)S(1)}, u32[]{:S(2)}, u32[]{:S(2)}) collective-permute-start(bf16[64,2048]{1,0:T(8,128)(2,1)S(1)} %get-tuple-element.29), channel_id=1, source_target_pairs={{4,0},{3,1},{6,2},{1,3},{0,4},{7,5},{2,6},{5,7},{12,8},{11,9},{14,... | collective-permute-start | bytes 786440 | tf_op jit(solution)/shard_map/ppermute | solution.py:359
  48.4 2.8 %routed_rows.2 = (bf16[64,2048]{1,0:T(8,128)(2,1)S(1)}, bf16[64,2048]{1,0:T(8,128)(2,1)S(1)}) custom-call(s32[2]{0:T(128)S(1)} %pad_add_fusion.place_ref, bf16[64,2176]{1,0:T(8,128)(2,1)} %collective-permute-done.5.first_ref, bf16[64,2176]{1,0:T(8,128)(2,1)S(1)} %join.1.second_ref, bf16[1,2048]{1,0:T(2,128)(2,1)S(1)} %broadcast_in_dim.20.branch_ref, ...), custom_call_target="tpu_custom_call" | custom-call | flops 805306368 | bytes 8388608 | tf_op jit(solution)/shard_map/routed_rows/pallas_call | solution.py:305
  51.2 1.6 %collective-permute-start.14 = (bf16[64,2048]{1,0:T(8,128)(2,1)S(1)}, bf16[64,2048]{1,0:T(8,128)(2,1)S(1)}, u32[]{:S(2)}, u32[]{:S(2)}) collective-permute-start(bf16[64,2048]{1,0:T(8,128)(2,1)S(1)} %get-tuple-element.30), channel_id=1, source_target_pairs={{6,0},{7,1},{4,2},{5,3},{2,4},{3,5},{0,6},{1,7},{14,8},{15,9},{12,... | collective-permute-start | bytes 786440 | tf_op jit(solution)/shard_map/ppermute | solution.py:359
  52.8 1.3 %collective-permute-done.18.far_ref = bf16[16,2176]{1,0:T(8,128)(2,1)S(1)} collective-permute-done((bf16[16,2176]{1,0:T(8,128)(2,1)S(1)}, bf16[16,2176]{1,0:T(8,128)(2,1)S(1)}, u32[]{:S(2)}, u32[]{:S(2)}) %collective-permute-start.18) | collective-permute-done | bytes 69664 | tf_op jit(solution)/shard_map/ppermute | solution.py:356
  54.1 1.3 %shared_mlp.1 = (bf16[16,2048]{1,0:T(8,128)(2,1)S(1)}, bf16[16,2048]{1,0:T(8,128)(2,1)S(1)}) custom-call(bf16[16,2176]{1,0:T(8,128)(2,1)S(1)} %mix.1.refs_0_.own_ref.packet_ref, bf16[16,2176]{1,0:T(8,128)(2,1)S(1)} %collective-permute-done.18.far_ref, bf16[2048,256]{1,0:T(8,128)(2,1)S(1)} %copy-done.4, bf16[2048,256]{1,0:T(8,128)(2,1)S(1)} %copy-done.5, ...), custom_call_target="tpu_custom_call" | custom-call | flops 100663296 | bytes 3145728 | tf_op jit(solution)/shard_map/shared_mlp/pallas_call | solution.py:452
  55.6 2.9 %collective-permute-done.14.refs_3_ = bf16[64,2048]{1,0:T(8,128)(2,1)S(1)} collective-permute-done((bf16[64,2048]{1,0:T(8,128)(2,1)S(1)}, bf16[64,2048]{1,0:T(8,128)(2,1)S(1)}, u32[]{:S(2)}, u32[]{:S(2)}) %collective-permute-start.14) | collective-permute-done | bytes 262176 | tf_op jit(solution)/shard_map/ppermute | solution.py:359
  58.8 2.7 %collective-permute-start.16 = (bf16[16,2048]{1,0:T(8,128)(2,1)S(1)}, bf16[16,2048]{1,0:T(8,128)(2,1)S(1)}, u32[]{:S(2)}, u32[]{:S(2)}) collective-permute-start(bf16[16,2048]{1,0:T(8,128)(2,1)S(1)} %get-tuple-element.33), channel_id=1, source_target_pairs={{16,0},{17,1},{18,2},{19,3},{20,4},{21,5},{22,6},{23,7},{24,8},{25... | collective-permute-start | bytes 196616 | tf_op jit(solution)/shard_map/ppermute | solution.py:359
  61.5 1.7 %collective-permute-start.17 = (bf16[16,2048]{1,0:T(8,128)(2,1)S(1)}, bf16[16,2048]{1,0:T(8,128)(2,1)S(1)}, u32[]{:S(2)}, u32[]{:S(2)}) collective-permute-start(bf16[16,2048]{1,0:T(8,128)(2,1)S(1)} %get-tuple-element.34), channel_id=1, source_target_pairs={{24,0},{25,1},{26,2},{27,3},{28,4},{29,5},{30,6},{31,7},{16,8},{17... | collective-permute-start | bytes 196616 | tf_op jit(solution)/shard_map/ppermute | solution.py:359
  63.3 1.2 %collective-permute-done.1.far_norm_ref = f32[2,1024]{1,0:T(2,128)S(1)} collective-permute-done((f32[2,1024]{1,0:T(2,128)S(1)}, f32[2,1024]{1,0:T(2,128)S(1)}, u32[]{:S(2)}, u32[]{:S(2)}) %collective-permute-start.1) | collective-permute-done | bytes 8224 | tf_op jit(solution)/shard_map/ppermute | solution.py:356
  64.4 1.0 %collective-permute-done.16.refs_2_ = bf16[16,2048]{1,0:T(8,128)(2,1)S(1)} collective-permute-done((bf16[16,2048]{1,0:T(8,128)(2,1)S(1)}, bf16[16,2048]{1,0:T(8,128)(2,1)S(1)}, u32[]{:S(2)}, u32[]{:S(2)}) %collective-permute-start.16) | collective-permute-done | bytes 65568 | tf_op jit(solution)/shard_map/ppermute | solution.py:359
  65.4 2.1 %collective-permute-done.17.refs_3_ = bf16[16,2048]{1,0:T(8,128)(2,1)S(1)} collective-permute-done((bf16[16,2048]{1,0:T(8,128)(2,1)S(1)}, bf16[16,2048]{1,0:T(8,128)(2,1)S(1)}, u32[]{:S(2)}, u32[]{:S(2)}) %collective-permute-start.17) | collective-permute-done | bytes 65568 | tf_op jit(solution)/shard_map/ppermute | solution.py:359
  67.8 1.2 %collective-permute-done.20.far_ref = bf16[16,1024]{1,0:T(8,128)(2,1)S(1)} collective-permute-done((bf16[16,1024]{1,0:T(8,128)(2,1)S(1)}, bf16[16,1024]{1,0:T(8,128)(2,1)S(1)}, u32[]{:S(2)}, u32[]{:S(2)}) %collective-permute-start.20) | collective-permute-done | bytes 32800 | tf_op jit(solution)/shard_map/ppermute | solution.py:356
  69.0 0.6 place.1
  (65 shorter events, 2.5 us)
Async XLA Ops:
  0.6 9.1 %copy-start.9 = (bf16[32,2048]{1,0:T(8,128)(2,1)S(1)}, bf16[32,2048]{1,0:T(8,128)(2,1)}, u32[]{:S(2)}) copy-start(bf16[32,2048]{1,0:T(8,128)(2,1)} %input_ref.1) | copy-start | bytes 393220
  0.7 9.1 %copy-start.8 = (bf16[512,512]{1,0:T(8,128)(2,1)S(1)}, bf16[512,512]{1,0:T(8,128)(2,1)}, u32[]{:S(2)}) copy-start(bf16[512,512]{1,0:T(8,128)(2,1)} %glu_ref.1) | copy-start | bytes 1572868
  0.7 9.1 %copy-start.12 = (f32[2048]{0:T(1024)S(1)}, f32[2048]{0:T(1024)}, u32[]{:S(2)}) copy-start(f32[2048]{0:T(1024)} %param.37) | copy-start | bytes 24580
  0.7 9.1 %copy-start.13 = (f32[2048]{0:T(1024)S(1)}, f32[2048]{0:T(1024)}, u32[]{:S(2)}) copy-start(f32[2048]{0:T(1024)} %param.38) | copy-start | bytes 24580
  0.7 31.5 %collective-permute-start.6 = (bf16[1,2048,256]{2,1,0:T(8,128)(2,1)}, bf16[1,2048,256]{2,1,0:T(8,128)(2,1)}, u32[]{:S(2)}, u32[]{:S(2)}) collective-permute-start(bf16[1,2048,256]{2,1,0:T(8,128)(2,1)} %refs_0_.3), channel_id=1, source_target_pairs={{0,1},{1,0},{2,3},{3,2},{4,5},{5,4},{6,7},{7,6},{8,9},{9,8},{10,11... | collective-permute-start | bytes 3145736 | tf_op jit(solution)/shard_map/ppermute | solution.py:356
  1.3 31.5 %collective-permute-start.7 = (bf16[1,2048,256]{2,1,0:T(8,128)(2,1)}, bf16[1,2048,256]{2,1,0:T(8,128)(2,1)}, u32[]{:S(2)}, u32[]{:S(2)}) collective-permute-start(bf16[1,2048,256]{2,1,0:T(8,128)(2,1)} %refs_1_.5), channel_id=1, source_target_pairs={{0,1},{1,0},{2,3},{3,2},{4,5},{5,4},{6,7},{7,6},{8,9},{9,8},{10,11... | collective-permute-start | bytes 3145736 | tf_op jit(solution)/shard_map/ppermute | solution.py:356
  1.3 31.4 %collective-permute-start.8 = (bf16[1,256,2048]{2,1,0:T(8,128)(2,1)}, bf16[1,256,2048]{2,1,0:T(8,128)(2,1)}, u32[]{:S(2)}, u32[]{:S(2)}) collective-permute-start(bf16[1,256,2048]{2,1,0:T(8,128)(2,1)} %refs_4_.5), channel_id=1, source_target_pairs={{0,1},{1,0},{2,3},{3,2},{4,5},{5,4},{6,7},{7,6},{8,9},{9,8},{10,11... | collective-permute-start | bytes 3145736 | tf_op jit(solution)/shard_map/ppermute | solution.py:356
  8.3 24.3 %copy-start.17 = (bf16[2048]{0:T(1024)(128)(2,1)S(1)}, bf16[2048]{0:T(1024)(128)(2,1)}, u32[]{:S(2)}) copy-start(bf16[2048]{0:T(1024)(128)(2,1)} %param.49) | copy-start | bytes 12292
  8.3 1.4 %collective-permute-start = (bf16[16,256]{1,0:T(8,128)(2,1)}, bf16[16,256]{1,0:T(8,128)(2,1)S(1)}, u32[]{:S(2)}, u32[]{:S(2)}) collective-permute-start(bf16[16,256]{1,0:T(8,128)(2,1)} %get-tuple-element.22), channel_id=1, source_target_pairs={{0,1},{1,0},{2,3},{3,2},{4,5},{5,4},{6,7},{7,6},{8,9},{9,8},{10,11... | collective-permute-start | bytes 24584 | tf_op jit(solution)/shard_map/ppermute | solution.py:356
  12.9 29.7 %copy-start = (bf16[1,2048,256]{2,1,0:T(8,128)(2,1)S(1)}, bf16[1,2048,256]{2,1,0:T(8,128)(2,1)}, u32[]{:S(2)}) copy-start(bf16[1,2048,256]{2,1,0:T(8,128)(2,1)} %refs_0_.3) | copy-start | bytes 3145732
  12.9 29.7 %copy-start.1 = (bf16[1,2048,256]{2,1,0:T(8,128)(2,1)S(1)}, bf16[1,2048,256]{2,1,0:T(8,128)(2,1)}, u32[]{:S(2)}) copy-start(bf16[1,2048,256]{2,1,0:T(8,128)(2,1)} %refs_1_.5) | copy-start | bytes 3145732
  12.9 29.6 %copy-start.2 = (bf16[1,256,2048]{2,1,0:T(8,128)(2,1)S(1)}, bf16[1,256,2048]{2,1,0:T(8,128)(2,1)}, u32[]{:S(2)}) copy-start(bf16[1,256,2048]{2,1,0:T(8,128)(2,1)} %refs_4_.5) | copy-start | bytes 3145732
  12.9 5.5 %collective-permute-start.2 = (bf16[16,2176]{1,0:T(8,128)(2,1)S(1)}, bf16[16,2176]{1,0:T(8,128)(2,1)S(1)}, u32[]{:S(2)}, u32[]{:S(2)}) collective-permute-start(bf16[16,2176]{1,0:T(8,128)(2,1)S(1)} %mix.1.refs_0_.own_ref.packet_ref), channel_id=1, source_target_pairs={{0,8},{1,9},{2,10},{3,11},{4,12},{5,13},{6,14},{7,15},{8,0},{9,1},... | collective-permute-start | bytes 208904 | tf_op jit(solution)/shard_map/ppermute | solution.py:359
  15.7 6.6 %collective-permute-start.3 = (bf16[16,2176]{1,0:T(8,128)(2,1)S(1)}, bf16[16,2176]{1,0:T(8,128)(2,1)S(1)}, u32[]{:S(2)}, u32[]{:S(2)}) collective-permute-start(bf16[16,2176]{1,0:T(8,128)(2,1)S(1)} %mix.1.refs_0_.own_ref.packet_ref), channel_id=1, source_target_pairs={{0,16},{1,17},{2,18},{3,19},{4,20},{5,21},{6,22},{7,23},{8,24},{9,... | collective-permute-start | bytes 208904 | tf_op jit(solution)/shard_map/ppermute | solution.py:359
  18.4 11.6 %collective-permute-start.9 = (bf16[64,1024]{1,0:T(8,128)(2,1)}, bf16[64,1024]{1,0:T(8,128)(2,1)S(1)}, u32[]{:S(2)}, u32[]{:S(2)}) collective-permute-start(bf16[64,1024]{1,0:T(8,128)(2,1)} %refs_7_.5), channel_id=1, source_target_pairs={{0,1},{1,0},{2,3},{3,2},{4,5},{5,4},{6,7},{7,6},{8,9},{9,8},{10,11... | collective-permute-start | bytes 393224 | tf_op jit(solution)/shard_map/ppermute | solution.py:356
  22.3 6.1 %collective-permute-start.4 = (bf16[16,2176]{1,0:T(8,128)(2,1)S(1)}, bf16[16,2176]{1,0:T(8,128)(2,1)S(1)}, u32[]{:S(2)}, u32[]{:S(2)}) collective-permute-start(bf16[16,2176]{1,0:T(8,128)(2,1)S(1)} %mix.1.refs_0_.own_ref.packet_ref), channel_id=1, source_target_pairs={{0,24},{1,25},{2,26},{3,27},{4,28},{5,29},{6,30},{7,31},{8,16},{9,... | collective-permute-start | bytes 208904 | tf_op jit(solution)/shard_map/ppermute | solution.py:359
  28.4 9.7 %collective-permute-start.10 = (bf16[64,2176]{1,0:T(8,128)(2,1)S(1)}, bf16[64,2176]{1,0:T(8,128)(2,1)}, u32[]{:S(2)}, u32[]{:S(2)}) collective-permute-start(bf16[64,2176]{1,0:T(8,128)(2,1)S(1)} %join.1.second_ref), channel_id=1, source_target_pairs={{0,2},{1,5},{2,0},{3,7},{4,6},{5,1},{6,4},{7,3},{8,10},{9,13},{10,... | collective-permute-start | bytes 835592 | tf_op jit(solution)/shard_map/ppermute | solution.py:359
  30.6 11.9 %collective-permute-start.11 = (bf16[64,2176]{1,0:T(8,128)(2,1)S(1)}, bf16[64,2176]{1,0:T(8,128)(2,1)}, u32[]{:S(2)}, u32[]{:S(2)}) collective-permute-start(bf16[64,2176]{1,0:T(8,128)(2,1)S(1)} %join.1.second_ref), channel_id=1, source_target_pairs={{0,4},{1,3},{2,6},{3,1},{4,0},{5,7},{6,2},{7,5},{8,12},{9,11},{10,... | collective-permute-start | bytes 835592 | tf_op jit(solution)/shard_map/ppermute | solution.py:359
  32.2 16.2 %collective-permute-start.5 = (bf16[64,2176]{1,0:T(8,128)(2,1)S(1)}, bf16[64,2176]{1,0:T(8,128)(2,1)}, u32[]{:S(2)}, u32[]{:S(2)}) collective-permute-start(bf16[64,2176]{1,0:T(8,128)(2,1)S(1)} %join.1.second_ref), channel_id=1, source_target_pairs={{0,6},{1,7},{2,4},{3,5},{4,2},{5,3},{6,0},{7,1},{8,14},{9,15},{10,... | collective-permute-start | bytes 835592 | tf_op jit(solution)/shard_map/ppermute | solution.py:359
  32.6 9.9 %copy-start.7 = (bf16[64,2048]{1,0:T(8,128)(2,1)S(1)}, bf16[64,2048]{1,0:T(8,128)(2,1)}, u32[]{:S(2)}) copy-start(bf16[64,2048]{1,0:T(8,128)(2,1)} %refs_6_.3) | copy-start | bytes 786436
  45.4 10.2 %collective-permute-start.12 = (bf16[64,2048]{1,0:T(8,128)(2,1)S(1)}, bf16[64,2048]{1,0:T(8,128)(2,1)S(1)}, u32[]{:S(2)}, u32[]{:S(2)}) collective-permute-start(bf16[64,2048]{1,0:T(8,128)(2,1)S(1)} %get-tuple-element.28), channel_id=1, source_target_pairs={{2,0},{5,1},{0,2},{7,3},{6,4},{1,5},{4,6},{3,7},{10,8},{13,9},{8,1... | collective-permute-start | bytes 786440 | tf_op jit(solution)/shard_map/ppermute | solution.py:359
  45.5 10.1 %collective-permute-start.13 = (bf16[64,2048]{1,0:T(8,128)(2,1)S(1)}, bf16[64,2048]{1,0:T(8,128)(2,1)S(1)}, u32[]{:S(2)}, u32[]{:S(2)}) collective-permute-start(bf16[64,2048]{1,0:T(8,128)(2,1)S(1)} %get-tuple-element.29), channel_id=1, source_target_pairs={{4,0},{3,1},{6,2},{1,3},{0,4},{7,5},{2,6},{5,7},{12,8},{11,9},{14,... | collective-permute-start | bytes 786440 | tf_op jit(solution)/shard_map/ppermute | solution.py:359
  51.2 12.0 %copy-start.18 = (f32[1024]{0:T(1024)S(1)}, f32[1024]{0:T(1024)}, u32[]{:S(2)}) copy-start(f32[1024]{0:T(1024)} %param.51) | copy-start | bytes 12292
  51.2 11.9 %copy-start.19 = (f32[1024]{0:T(1024)S(1)}, f32[1024]{0:T(1024)}, u32[]{:S(2)}) copy-start(f32[1024]{0:T(1024)} %param.50) | copy-start | bytes 12292
  51.2 7.3 %collective-permute-start.14 = (bf16[64,2048]{1,0:T(8,128)(2,1)S(1)}, bf16[64,2048]{1,0:T(8,128)(2,1)S(1)}, u32[]{:S(2)}, u32[]{:S(2)}) collective-permute-start(bf16[64,2048]{1,0:T(8,128)(2,1)S(1)} %get-tuple-element.30), channel_id=1, source_target_pairs={{6,0},{7,1},{4,2},{5,3},{2,4},{3,5},{0,6},{1,7},{14,8},{15,9},{12,... | collective-permute-start | bytes 786440 | tf_op jit(solution)/shard_map/ppermute | solution.py:359
  52.8 1.3 %collective-permute-start.18 = (bf16[16,2176]{1,0:T(8,128)(2,1)S(1)}, bf16[16,2176]{1,0:T(8,128)(2,1)S(1)}, u32[]{:S(2)}, u32[]{:S(2)}) collective-permute-start(bf16[16,2176]{1,0:T(8,128)(2,1)S(1)} %mix.1.refs_0_.own_ref.packet_ref), channel_id=1, source_target_pairs={{0,1},{1,0},{2,3},{3,2},{4,5},{5,4},{6,7},{7,6},{8,9},{9,8},{10,11... | collective-permute-start | bytes 208904 | tf_op jit(solution)/shard_map/ppermute | solution.py:356
  55.4 9.0 %collective-permute-start.19 = (bf16[16,2048]{1,0:T(8,128)(2,1)S(1)}, bf16[16,2048]{1,0:T(8,128)(2,1)S(1)}, u32[]{:S(2)}, u32[]{:S(2)}) collective-permute-start(bf16[16,2048]{1,0:T(8,128)(2,1)S(1)} %get-tuple-element.36), channel_id=1, source_target_pairs={{0,1},{1,0},{2,3},{3,2},{4,5},{5,4},{6,7},{7,6},{8,9},{9,8},{10,11... | collective-permute-start | bytes 196616 | tf_op jit(solution)/shard_map/ppermute | solution.py:356
  58.7 5.7 %collective-permute-start.15 = (bf16[16,2048]{1,0:T(8,128)(2,1)S(1)}, bf16[16,2048]{1,0:T(8,128)(2,1)S(1)}, u32[]{:S(2)}, u32[]{:S(2)}) collective-permute-start(bf16[16,2048]{1,0:T(8,128)(2,1)S(1)} %get-tuple-element.32), channel_id=1, source_target_pairs={{8,0},{9,1},{10,2},{11,3},{12,4},{13,5},{14,6},{15,7},{0,8},{1,9},... | collective-permute-start | bytes 196616 | tf_op jit(solution)/shard_map/ppermute | solution.py:359
  58.8 6.6 %collective-permute-start.16 = (bf16[16,2048]{1,0:T(8,128)(2,1)S(1)}, bf16[16,2048]{1,0:T(8,128)(2,1)S(1)}, u32[]{:S(2)}, u32[]{:S(2)}) collective-permute-start(bf16[16,2048]{1,0:T(8,128)(2,1)S(1)} %get-tuple-element.33), channel_id=1, source_target_pairs={{16,0},{17,1},{18,2},{19,3},{20,4},{21,5},{22,6},{23,7},{24,8},{25... | collective-permute-start | bytes 196616 | tf_op jit(solution)/shard_map/ppermute | solution.py:359
  61.5 6.1 %collective-permute-start.17 = (bf16[16,2048]{1,0:T(8,128)(2,1)S(1)}, bf16[16,2048]{1,0:T(8,128)(2,1)S(1)}, u32[]{:S(2)}, u32[]{:S(2)}) collective-permute-start(bf16[16,2048]{1,0:T(8,128)(2,1)S(1)} %get-tuple-element.34), channel_id=1, source_target_pairs={{24,0},{25,1},{26,2},{27,3},{28,4},{29,5},{30,6},{31,7},{16,8},{17... | collective-permute-start | bytes 196616 | tf_op jit(solution)/shard_map/ppermute | solution.py:359
  63.2 1.2 %collective-permute-start.1 = (f32[2,1024]{1,0:T(2,128)S(1)}, f32[2,1024]{1,0:T(2,128)S(1)}, u32[]{:S(2)}, u32[]{:S(2)}) collective-permute-start(f32[2,1024]{1,0:T(2,128)S(1)} %pad_maximum_fusion.own_norm_ref), channel_id=1, source_target_pairs={{0,1},{1,0},{2,3},{3,2},{4,5},{5,4},{6,7},{7,6},{8,9},{9,8},{10,11... | collective-permute-start | bytes 24584 | tf_op jit(solution)/shard_map/ppermute | solution.py:356
  67.7 1.3 %collective-permute-start.20 = (bf16[16,1024]{1,0:T(8,128)(2,1)S(1)}, bf16[16,1024]{1,0:T(8,128)(2,1)S(1)}, u32[]{:S(2)}, u32[]{:S(2)}) collective-permute-start(bf16[16,1024]{1,0:T(8,128)(2,1)S(1)} %get-tuple-element.38), channel_id=1, source_target_pairs={{0,1},{1,0},{2,3},{3,2},{4,5},{5,4},{6,7},{7,6},{8,9},{9,8},{10,11... | collective-permute-start | bytes 98312 | tf_op jit(solution)/shard_map/ppermute | solution.py:356
  (9 other events, 45.3 us)
